TPU v7x, 32 devices: a whole 2x2x4 slice. The times are simulated.
32 devices in a mesh: grp: 2 (over y), sp: 4 (over z), tp: 4 (over x, core).
Axes of the slice: x: 2, y: 2, z: 4, core: 2. Of those that a mesh axis runs over, the one named last changes fastest.
Arguments:
- stream: bfloat16 [3072, 4096], P(('grp', 'sp'), 'tp'), parts along dimension 0, may hold values from -6 to 6
- norm_gain: bfloat16 [2, 4096], replicated, may hold values from 0.099609375 to 1.8984375
- w_signal: bfloat16 [2, 4096, 1024], P(None, 'sp', 'tp'), may hold values from -0.09375 to 0.09375
- w_gate: bfloat16 [2, 4096, 1024], P(None, 'sp', 'tp'), may hold values from -0.09375 to 0.09375
- conv_taps: bfloat16 [2, 31, 1024], P(None, None, 'tp'), may hold values from -4 to 4
- conv_bias: bfloat16 [2, 1024], P(None, 'tp'), may hold values from -3 to 3
- ln_gain: bfloat16 [2, 1024], P(None, 'tp'), may hold values from 0.099609375 to 1.8984375
- ln_shift: bfloat16 [2, 1024], P(None, 'tp'), may hold values from -3 to 3
- w_out: bfloat16 [2, 1024, 4096], P(None, 'sp', 'tp'), may hold values from -0.375 to 0.375
Outputs:
- mixed_stream: bfloat16 [3072, 4096], P(('grp', 'sp'), 'tp'), parts along dimension 0
There are 2 independent parts, one for each index of `grp`. A program takes and returns all parts, laid end to end along the dimension named above; an argument that names none is the same for every part. Nothing has to cross between parts.
All inputs are finite; a program needn't handle non-finite values.
Results may differ from a plain program's by a relative error of at most 0.01.
Values may be sent and summed in bfloat16 or wider, within the bound.
A program may use at most 64 MiB of HBM per device.

v0:
```python
import functools

import jax
import jax.numpy as jnp
from jax import lax
from jax.experimental import pallas as pl
from jax.experimental.pallas import tpu as pltpu
from jax.sharding import PartitionSpec as P

MESH = pl.DeviceIdType.MESH
EPS = 1e-05
F32 = jnp.float32
BF16 = jnp.bfloat16
SIG, GATE, OUT = 0, 1, 2
CHUNK = 32
PIECES = 2


def sigmoid(v):
    return 1.0 / (1.0 + jnp.exp(-v))


def kernel(
    sizes,
    stream, gain, w_signal, w_gate, taps, bias, ln_gain, ln_shift, w_out,
    result,
    sig_all, gate_all, out_all, feats, scaled_feats, inv, acc_sig, acc_gate,
    tail, halo, padded, filt, stat_cols, stat_rows, acts,
    load_sem, stream_sem, own_send, z_send, z_recv, y_send, y_recv,
    cross_send, cross_recv, core_send, core_recv,
    halo_send, halo_recv, stat_send, stat_recv,
):
    groups, sp, tp, layers, rows, kernel_taps, hp, width, channels = sizes
    g, s, t = lax.axis_index("grp"), lax.axis_index("sp"), lax.axis_index("tp")
    chips = tp // 2
    core, chip = lax.rem(t, 2), lax.div(t, 2)
    mate = t + 1 - 2 * core
    share = sp // tp
    banks = (sig_all, gate_all, out_all)
    held = (w_signal, w_gate, w_out)

    inner = (s > 0) & (s < sp - 1)
    pieces = [w.shape[2] for w in held]

    def load(l, k):
        return pltpu.make_async_copy(held[k].at[l], banks[k].at[l, s], load_sem.at[l, k])

    own_stream = pltpu.make_async_copy(stream, feats.at[0, t], stream_sem)
    own_stream.start()
    for l in range(layers):
        for k in range(3):
            load(l, k).start()

    barrier = pltpu.get_barrier_semaphore()

    def greet(where):
        pl.semaphore_signal(barrier, inc=1, device_id=where, device_id_type=MESH)

    @pl.when(s > 0)
    def _():
        greet({"sp": s - 1})

    @pl.when(s < sp - 1)
    def _():
        greet({"sp": s + 1})

    for i in range(1, groups):
        greet({"grp": lax.rem(g + i, groups)})
    for i in range(1, tp):
        greet({"tp": lax.rem(t + i, tp)})
    pl.semaphore_wait(
        barrier,
        jnp.where(s > 0, 1, 0) + jnp.where(s < sp - 1, 1, 0) + (groups - 1 + tp - 1),
    )

    def z_copy(l, k, q, shard, way, mine=False):
        ref = banks[k].at[l, shard, g, q]
        return pltpu.make_async_remote_copy(
            src_ref=ref, dst_ref=ref,
            send_sem=own_send.at[l, k, q] if mine and way else z_send.at[l, k, q, shard],
            recv_sem=z_recv.at[l, k, q, shard],
            device_id={"sp": s + 1 if way == 0 else s - 1}, device_id_type=MESH,
        )

    def y_copy(l, k, q, shard, half, where):
        ref = banks[k].at[l, shard, half, q]
        return pltpu.make_async_remote_copy(
            src_ref=ref, dst_ref=ref,
            send_sem=y_send.at[l, k, q, shard], recv_sem=y_recv.at[l, k, q, shard],
            device_id=where, device_id_type=MESH,
        )

    def own(l, k, done=False):
        if not done:
            load(l, k).wait()
        for way, there, end in ((0, s < sp - 1, s == 0), (1, s > 0, s == sp - 1)):
            @pl.when(there)
            def _(way=way, end=end):
                for q in range(pieces[k]):
                    copy = z_copy(l, k, q, s, way, True)
                    copy.wait_send() if done else copy.start()

                @pl.when(end)
                def _():
                    for q in range(pieces[k]):
                        where = {"sp": s + 1 if way == 0 else s - 1}
                        copy = y_copy(l, k, q, s, 1 - g, where)
                        copy.wait_send() if done else copy.start()

    def sides(d):
        left, right = s - 1 - d, s + 1 + d
        return (
            (0, left, left >= 0, s < sp - 1, (left > 0) | (d > 0)),
            (1, right, right <= sp - 1, s > 0, (right < sp - 1) | (d > 0)),
        )

    def relay(l, k, d, done=False):
        for way, shard, here, onward, across in sides(d):
            @pl.when(here)
            def _(way=way, shard=shard, onward=onward, across=across):
                for q in range(pieces[k]):
                    if not done:
                        z_copy(l, k, q, shard, way).wait_recv()

                    @pl.when(onward)
                    def _():
                        copy = z_copy(l, k, q, shard, way)
                        copy.wait_send() if done else copy.start()

                    @pl.when(across)
                    def _():
                        copy = y_copy(l, k, q, shard, g, {"grp": 1 - g})
                        copy.wait_send() if done else copy.start()

    def other_half(l, k, d):
        for _, shard, here, _, _ in sides(d):
            @pl.when(here)
            def _(shard=shard):
                for q in range(pieces[k]):
                    y_copy(l, k, q, shard, 1 - g, {"grp": 1 - g}).wait_recv()

    def cross_copy(buf, n, block, i):
        ref = buf.at[block]
        return pltpu.make_async_remote_copy(
            src_ref=ref, dst_ref=ref,
            send_sem=cross_send.at[n, i], recv_sem=cross_recv.at[n, block],
            device_id={"tp": lax.rem(chip + i, chips) * 2 + core}, device_id_type=MESH,
        )

    def core_copy(buf, n, block):
        ref = buf.at[block]
        return pltpu.make_async_remote_copy(
            src_ref=ref, dst_ref=ref,
            send_sem=core_send.at[n, block], recv_sem=core_recv.at[n, block],
            device_id={"tp": mate}, device_id_type=MESH,
        )

    def spread_start(buf, n):
        for i in range(1, chips):
            cross_copy(buf, n, t, i).start()
        core_copy(buf, n, t).start()

    def spread_relay(buf, n):
        for i in range(1, chips):
            block = lax.rem(chip + i, chips) * 2 + core
            cross_copy(buf, n, block, i).wait_recv()
            core_copy(buf, n, block).start()

    def spread_wait(buf, n):
        for j in range(chips):
            core_copy(buf, n, j * 2 + 1 - core).wait_recv()

    def spread_done(buf, n):
        for i in range(1, chips):
            cross_copy(buf, n, t, i).wait_send()
        for j in range(chips):
            core_copy(buf, n, j * 2 + core).wait_send()

    def stat_copy(l, i, block):
        return pltpu.make_async_remote_copy(
            src_ref=stat_rows.at[l, block], dst_ref=stat_rows.at[l, block],
            send_sem=stat_send.at[l, i], recv_sem=stat_recv.at[l, block],
            device_id={"tp": lax.rem(t + i, tp)}, device_id_type=MESH,
        )

    def halo_copy(l):
        return pltpu.make_async_remote_copy(
            src_ref=tail.at[l], dst_ref=halo.at[l],
            send_sem=halo_send.at[l], recv_sem=halo_recv.at[l],
            device_id={"sp": s + 1}, device_id_type=MESH,
        )

    def normalise(l):
        part = width // tp

        def body(c, carry):
            at = pl.ds(pl.multiple_of(c * CHUNK, CHUNK), CHUNK)
            total = jnp.zeros((CHUNK, 1), F32)
            for b in range(tp):
                x = feats[l, b, at, :].astype(F32)
                total = total + jnp.sum(x * x, axis=1, keepdims=True)
                scaled_feats[b, at, :] = (
                    x * gain[l : l + 1, b * part : (b + 1) * part].astype(F32)
                ).astype(BF16)
            inv[at, :] = jnp.broadcast_to(lax.rsqrt(total / width + EPS), (CHUNK, 128))
            return carry

        lax.fori_loop(0, rows // CHUNK, body, 0)

    local = channels // tp

    def project(l):
        for k, acc in ((SIG, acc_sig), (GATE, acc_gate)):
            def body(b, carry, k=k, acc=acc):
                w = banks[k][l, pl.ds(b * share, share)].reshape(width // tp, local)
                acc[...] += jnp.dot(scaled_feats[b], w, preferred_element_type=F32)
                return carry

            acc[...] = jnp.zeros_like(acc)
            for d in range(sp - 1):
                other_half(l, k, d)
            lax.fori_loop(0, tp, body, 0)

        def blend(c, carry):
            at = pl.ds(pl.multiple_of(c * CHUNK, CHUNK), CHUNK)
            r = inv[at, 0:1]
            v = (acc_sig[at, :] * r) * sigmoid(acc_gate[at, :] * r)
            to = pl.ds(pl.multiple_of(hp + c * CHUNK, 8), CHUNK)
            padded[to, :] = v.astype(BF16).astype(F32)
            return carry

        lax.fori_loop(0, rows // CHUNK, blend, 0)
        tail[l] = padded[rows : rows + hp, :].astype(BF16)

        @pl.when(s < sp - 1)
        def _():
            halo_copy(l).start()

    def convolve(l):
        def settle():
            @pl.when(s > 0)
            def _():
                halo_copy(l).wait_recv()
                padded[0:hp, :] = halo[l].astype(F32)

            @pl.when(s == 0)
            def _():
                padded[0:hp, :] = jnp.zeros((hp, local), F32)

        tap_rows = taps[:, l, :].astype(F32)
        first = hp - (kernel_taps - 1)
        lane = lax.broadcasted_iota(jnp.int32, (CHUNK, 128), 1)
        for c in [*range(1, rows // CHUNK), 0]:
            if c == 0:
                settle()
            low = c * CHUNK
            total = jnp.broadcast_to(bias[l : l + 1, :].astype(F32), (CHUNK, local))
            for j in range(kernel_taps):
                start = low + first + j
                total = total + tap_rows[j : j + 1, :] * padded[start : start + CHUNK, :]
            filt[low : low + CHUNK, :] = total
            one = jnp.sum(total, axis=1, keepdims=True)
            two = jnp.sum(total * total, axis=1, keepdims=True)
            stat_cols[low : low + CHUNK, :] = jnp.where(
                lane == 0, one, jnp.where(lane == 1, two, 0.0)
            )
        stat_rows[l, t] = jnp.transpose(stat_cols[...])[0:8, :]
        for i in range(1, tp):
            stat_copy(l, i, t).start()

    def activate(l):
        for i in range(1, tp):
            stat_copy(l, i, lax.rem(t + i, tp)).wait_recv()
        sums = jnp.sum(stat_rows[l], axis=0)
        stat_cols[...] = jnp.transpose(
            jnp.concatenate([sums, jnp.zeros((120, rows), F32)], axis=0)
        )
        gains, shifts = ln_gain[l : l + 1, :].astype(F32), ln_shift[l : l + 1, :].astype(F32)

        def body(c, carry):
            at = pl.ds(pl.multiple_of(c * CHUNK, CHUNK), CHUNK)
            average = stat_cols[at, 0:1] / channels
            spread = stat_cols[at, 1:2] / channels - average * average
            v = (filt[at, :] - average) * lax.rsqrt(spread + EPS) * gains + shifts
            acts[l, t, at, :] = (v * sigmoid(v)).astype(BF16)
            return carry

        lax.fori_loop(0, rows // CHUNK, body, 0)

    def update(l):
        columns = width // tp
        tile = min(256, columns)
        deep = 128

        def body(c, carry):
            at = pl.ds(pl.multiple_of(c * deep, deep), deep)
            for n in range(columns // tile):
                cut = slice(n * tile, (n + 1) * tile)
                total = feats[l, t, at, cut].astype(F32)
                for b in range(tp):
                    w = out_all[l, b * share : (b + 1) * share, :, :, :, cut].reshape(local, tile)
                    total = total + jnp.dot(acts[l, b, at, :], w, preferred_element_type=F32)
                if l + 1 < layers:
                    feats[l + 1, t, at, cut] = total.astype(BF16)
                else:
                    result[at, cut] = total.astype(BF16)
            return carry

        lax.fori_loop(0, rows // deep, body, 0)

    hops = range(sp - 1)
    own(0, SIG)
    own(0, GATE)
    own_stream.wait()
    spread_start(feats.at[0], 0)
    for l in range(layers):
        x_cut = [(d, k) for d in hops for k in (SIG, GATE)]
        middle = len(x_cut) - 3 if l == 0 else len(x_cut) - 2
        for i, (d, k) in enumerate(x_cut):
            if l and i == 0:
                continue
            if i == middle:
                if l:
                    own(l, OUT)
                spread_relay(feats.at[l], 2 * l)
            relay(l, k, d)
        if l == 0:
            own(l, OUT)
        spread_wait(feats.at[l], 2 * l)
        normalise(l)
        project(l)

        @pl.when(inner)
        def _(l=l):
            for d in hops:
                relay(l, OUT, d)

        if l + 1 < layers:
            own(l + 1, SIG)
            own(l + 1, GATE)
        convolve(l)

        @pl.when(jnp.logical_not(inner))
        def _(l=l):
            for d in hops:
                relay(l, OUT, d)

        activate(l)
        spread_start(acts.at[l], 2 * l + 1)
        if l + 1 < layers:
            relay(l + 1, SIG, 0)
        spread_relay(acts.at[l], 2 * l + 1)
        for d in hops:
            other_half(l, OUT, d)
        spread_wait(acts.at[l], 2 * l + 1)
        update(l)
        if l + 1 < layers:
            spread_start(feats.at[l + 1], 2 * l + 2)

    for l in range(layers):
        for k in (SIG, GATE, OUT):
            own(l, k, done=True)
            for d in hops:
                relay(l, k, d, done=True)
        spread_done(feats.at[l], 2 * l)
        spread_done(acts.at[l], 2 * l + 1)
        for i in range(1, tp):
            stat_copy(l, i, t).wait_send()

        @pl.when(s < sp - 1)
        def _(l=l):
            halo_copy(l).wait_send()


def shards(counts, stream, norm_gain, w_signal, w_gate, conv_taps, conv_bias, ln_gain, ln_shift, w_out):
    groups, sp, tp = counts
    layers, deep, local = w_signal.shape
    rows, part = stream.shape
    kernel_taps = conv_taps.shape[1]
    hp = -(-(kernel_taps - 1) // 16) * 16
    width, channels = part * tp, local * tp

    def cut(w):
        half = w.shape[1] // groups
        count = PIECES if half % (16 * PIECES) == 0 else 1
        return w.reshape(layers, groups, count, half // count, w.shape[2])

    w_signal, w_gate, w_out = cut(w_signal), cut(w_gate), cut(w_out)
    bank = lambda w: pltpu.VMEM((layers, sp) + w.shape[1:], BF16)
    most = max(w.shape[2] for w in (w_signal, w_gate, w_out))
    line = (layers, 3, most, sp)
    dma = lambda *shape: pltpu.SemaphoreType.DMA(shape)
    anywhere = pl.BlockSpec(memory_space=pl.ANY)
    inside = pl.BlockSpec(memory_space=pltpu.VMEM)
    return pl.pallas_call(
        functools.partial(
            kernel, (groups, sp, tp, layers, rows, kernel_taps, hp, width, channels)
        ),
        out_shape=jax.ShapeDtypeStruct(stream.shape, BF16),
        in_specs=[anywhere, inside, anywhere, anywhere, inside, inside, inside, inside, anywhere],
        out_specs=inside,
        scratch_shapes=[
            bank(w_signal), bank(w_gate), bank(w_out),
            pltpu.VMEM((layers, tp, rows, part), BF16),
            pltpu.VMEM((tp, rows, part), BF16),
            pltpu.VMEM((rows, 128), F32),
            pltpu.VMEM((rows, local), F32),
            pltpu.VMEM((rows, local), F32),
            pltpu.VMEM((layers, hp, local), BF16),
            pltpu.VMEM((layers, hp, local), BF16),
            pltpu.VMEM((hp + rows, local), F32),
            pltpu.VMEM((rows, local), F32),
            pltpu.VMEM((rows, 128), F32),
            pltpu.VMEM((layers, tp, 8, rows), F32),
            pltpu.VMEM((layers, tp, rows, local), BF16),
            dma(layers, 3), pltpu.SemaphoreType.DMA,
            dma(layers, 3, most), dma(*line), dma(*line), dma(*line), dma(*line),
            dma(2 * layers, tp), dma(2 * layers, tp), dma(2 * layers, tp), dma(2 * layers, tp),
            dma(layers), dma(layers), dma(layers, tp), dma(layers, tp),
        ],
        compiler_params=pltpu.CompilerParams(
            collective_id=0, has_side_effects=True, vmem_limit_bytes=60 * 1024 * 1024
        ),
    )(
        stream, norm_gain, w_signal, w_gate, jnp.transpose(conv_taps, (1, 0, 2)), conv_bias,
        ln_gain, ln_shift, w_out,
    )


def solution(mesh):
    counts = tuple(mesh.shape[name] for name in ("grp", "sp", "tp"))
    return jax.shard_map(
        functools.partial(shards, counts),
        mesh=mesh,
        in_specs=(
            P(("grp", "sp"), "tp"),
            P(),
            P(None, "sp", "tp"),
            P(None, "sp", "tp"),
            P(None, None, "tp"),
            P(None, "tp"),
            P(None, "tp"),
            P(None, "tp"),
            P(None, "sp", "tp"),
        ),
        out_specs=P(("grp", "sp"), "tp"),
        check_vma=False,
    )
```

profile of v0, /device:TPU:0, one launch (start us, length us, event | category | flops | bytes accessed | tf_op | source)
XLA Modules:
  0.0 135.5 jit_solution(4683719726377451037)
XLA Ops:
  0.0 133.5 %shard_map.91 = bf16[384,1024]{1,0:T(8,128)(2,1)} custom-call(bf16[384,1024]{1,0:T(8,128)(2,1)} %stream.1, bf16[2,4096]{1,0:T(2,128)(2,1)} %gain.1, bf16[2,2,2,256,256]{4,3,2,1,0:T(8,128)(2,1)} %bitcast.4, bf16[2,2,2,256,256]{4,3,2,1,0:T(8,128)(2,1)} %bitcast.5, bf16[31,2,256]{2,1,0:T(2,128)(2,1)} %bitcast.7, bf16[2,256]{1,0:T(2,128)(2,1)} %bias.1, ...), custom_call_target="tpu_custom_call" | custom-call | tf_op jit(solution)/shard_map/pallas_call | solution.py:395
  133.5 2.1 %copy.11 = bf16[384,1024]{1,0:T(8,128)(2,1)} copy(bf16[384,1024]{1,0:T(8,128)(2,1)} %shard_map.91) | data formatting | bytes 1572864
where the time goes:
time: 136 us
  Pallas kernels  133 us (98%)
  local copies, waits for them, and re-layouts  2.06 us (2%)
    pallas_call x1, Pallas kernels, shards(): pl.pallas_call(functools.partial(kernel, (groups, sp, tp, layers, rows, k...  133 us

commit v1 on v0

--- a/solution.py
+++ b/solution.py
@@ -372,6 +372,590 @@
             halo_copy(l).wait_send()
 
 
+def direct(l, k, q, count):
+    return l > 0 or k == OUT or q < count - 1 or count == 1
+
+
+def fold_kernel(
+    sizes,
+    stream, gain, w_signal, w_gate, taps, bias, ln_gain, ln_shift, w_out,
+    result,
+    sig_all, gate_all, out_all, feats, far, scaled, squares, acc_sig, acc_gate,
+    back, tail, halo, padded, filt, stat_cols, stat_rows, acts,
+    load_sem, stream_sem, z_send, end_send, z_recv, y_send, y_recv,
+    cross_send, cross_recv, core_send, core_recv,
+    far_send, far_recv, back_send, back_recv,
+    halo_send, halo_recv, stat_send, stat_recv,
+):
+    groups, sp, tp, layers, rows, kernel_taps, hp, width, channels = sizes
+    g, s, t = lax.axis_index("grp"), lax.axis_index("sp"), lax.axis_index("tp")
+    chips = tp // 2
+    core, chip = lax.rem(t, 2), lax.div(t, 2)
+    mate = t + 1 - 2 * core
+    last, middle = sp - 1, sp // 2
+    outer = (s == 0) | (s == last)
+    inner = jnp.logical_not(outer)
+    pair = s + 1 - 2 * lax.rem(s, 2)
+    mid = jnp.where(outer, pair, s)
+    end = jnp.where(outer, s, pair)
+    mid2, end2 = last - mid, last - end
+    banks = (sig_all, gate_all, out_all)
+    held = (w_signal, w_gate, w_out)
+    pieces = [w.shape[2] for w in held]
+    local, part = channels // tp, width // tp
+    parts = ((128, rows - 128), (0, 128))
+    both = range(len(parts))
+    other_group = {"grp": 1 - g}
+
+    def load(l, k):
+        return pltpu.make_async_copy(held[k].at[l], banks[k].at[l, s], load_sem.at[l, k])
+
+    own_stream = pltpu.make_async_copy(stream, feats.at[0, t], stream_sem)
+    own_stream.start()
+    for l in range(layers):
+        for k in range(3):
+            load(l, k).start()
+
+    barrier = pltpu.get_barrier_semaphore()
+
+    def greet(where):
+        pl.semaphore_signal(barrier, inc=1, device_id=where, device_id_type=MESH)
+
+    @pl.when(s > 0)
+    def _():
+        greet({"sp": s - 1})
+
+    @pl.when(s < last)
+    def _():
+        greet({"sp": s + 1})
+
+    for i in range(1, groups):
+        greet({"grp": lax.rem(g + i, groups)})
+    for i in range(1, tp):
+        greet({"tp": lax.rem(t + i, tp)})
+    pl.semaphore_wait(
+        barrier,
+        jnp.where(s > 0, 1, 0) + jnp.where(s < last, 1, 0) + (groups - 1 + tp - 1),
+    )
+
+    def z_copy(l, k, q, shard, to, sems):
+        ref = banks[k].at[l, shard, g, q]
+        return pltpu.make_async_remote_copy(
+            src_ref=ref, dst_ref=ref,
+            send_sem=sems.at[l, k, q, shard], recv_sem=z_recv.at[l, k, q, shard],
+            device_id={"sp": to}, device_id_type=MESH,
+        )
+
+    def y_copy(l, k, q, shard, half, where):
+        ref = banks[k].at[l, shard, half, q]
+        return pltpu.make_async_remote_copy(
+            src_ref=ref, dst_ref=ref,
+            send_sem=y_send.at[l, k, q, shard], recv_sem=y_recv.at[l, k, q, shard],
+            device_id=where, device_id_type=MESH,
+        )
+
+    def flow(copy, done):
+        copy.wait_send() if done else copy.start()
+
+    def across(l, k, q, shard, done=False):
+        flow(y_copy(l, k, q, shard, g, other_group), done)
+
+    def to_end(l, k, q, shard, done=False):
+        flow(z_copy(l, k, q, shard, end, end_send), done)
+
+    def to_middle(l, k, q, shard, done=False):
+        flow(z_copy(l, k, q, shard, mid2, z_send), done)
+
+    def lift(l, k, q, done=False):
+        flow(z_copy(l, k, q, s, mid, z_send), done)
+
+    def lift_other(l, k, q, done=False):
+        if direct(l, k, q, pieces[k]):
+            flow(y_copy(l, k, q, s, 1 - g, {"sp": mid}), done)
+
+    def arrived(l, k, q, shard):
+        z_copy(l, k, q, shard, mid, z_send).wait_recv()
+
+    def each(l, kinds, act):
+        for k in kinds:
+            for q in range(pieces[k]):
+                act(l, k, q)
+
+    def pass_on(l, k, q):
+        arrived(l, k, q, end)
+        to_middle(l, k, q, end)
+        if not direct(l, k, q, pieces[k]):
+            across(l, k, q, end)
+
+    def take(shard, onward=True):
+        def act(l, k, q):
+            arrived(l, k, q, shard)
+            across(l, k, q, shard)
+            if onward:
+                to_end(l, k, q, shard)
+        return act
+
+    def onward(shard):
+        return lambda l, k, q: to_end(l, k, q, shard)
+
+    def ready(l, k, shard):
+        for q in range(pieces[k]):
+            y_copy(l, k, q, shard, 1 - g, other_group).wait_recv()
+
+    def ready_all(l, k):
+        for shard in (pair, mid2, end2):
+            ready(l, k, shard)
+
+    def rows_of(h):
+        return pl.ds(parts[h][0], parts[h][1])
+
+    def cross_copy(buf, n, h, block, i):
+        ref = buf.at[block, rows_of(h)]
+        return pltpu.make_async_remote_copy(
+            src_ref=ref, dst_ref=ref,
+            send_sem=cross_send.at[n, h, i], recv_sem=cross_recv.at[n, h, block],
+            device_id={"tp": lax.rem(chip + i, chips) * 2 + core}, device_id_type=MESH,
+        )
+
+    def core_copy(buf, n, h, block):
+        ref = buf.at[block, rows_of(h)]
+        return pltpu.make_async_remote_copy(
+            src_ref=ref, dst_ref=ref,
+            send_sem=core_send.at[n, h, block], recv_sem=core_recv.at[n, h, block],
+            device_id={"tp": mate}, device_id_type=MESH,
+        )
+
+    def spread_start(buf, n, h):
+        for i in range(1, chips):
+            cross_copy(buf, n, h, t, i).start()
+        core_copy(buf, n, h, t).start()
+
+    def spread_relay(buf, n, h):
+        for i in range(1, chips):
+            block = lax.rem(chip + i, chips) * 2 + core
+            cross_copy(buf, n, h, block, i).wait_recv()
+            core_copy(buf, n, h, block).start()
+
+    def spread_near(buf, n, h):
+        core_copy(buf, n, h, mate).wait_recv()
+
+    def spread_rest(buf, n, h):
+        for i in range(1, chips):
+            core_copy(buf, n, h, lax.rem(chip + i, chips) * 2 + 1 - core).wait_recv()
+
+    def spread_done(buf, n):
+        for h in both:
+            for i in range(1, chips):
+                cross_copy(buf, n, h, t, i).wait_send()
+            for j in range(chips):
+                core_copy(buf, n, h, j * 2 + core).wait_send()
+
+    far_blocks = [lax.rem(chip + i, chips) * 2 + c for i in range(1, chips) for c in (core, 1 - core)]
+    near_blocks = [t, mate]
+
+    def far_copy(h):
+        return pltpu.make_async_remote_copy(
+            src_ref=feats.at[0, t, rows_of(h)], dst_ref=far.at[t, rows_of(h)],
+            send_sem=far_send.at[h], recv_sem=far_recv.at[h],
+            device_id={"sp": mid}, device_id_type=MESH,
+        )
+
+    def back_copy(h):
+        ref = back.at[rows_of(h)]
+        return pltpu.make_async_remote_copy(
+            src_ref=ref, dst_ref=ref,
+            send_sem=back_send.at[h], recv_sem=back_recv.at[h],
+            device_id={"sp": end}, device_id_type=MESH,
+        )
+
+    def stat_copy(l, h, i, block):
+        ref = stat_rows.at[l, block, :, rows_of(h)]
+        return pltpu.make_async_remote_copy(
+            src_ref=ref, dst_ref=ref,
+            send_sem=stat_send.at[l, h, i], recv_sem=stat_recv.at[l, h, block],
+            device_id={"tp": lax.rem(t + i, tp)}, device_id_type=MESH,
+        )
+
+    def halo_copy(l):
+        return pltpu.make_async_remote_copy(
+            src_ref=tail.at[l], dst_ref=halo.at[l],
+            send_sem=halo_send.at[l], recv_sem=halo_recv.at[l],
+            device_id={"sp": s + 1}, device_id_type=MESH,
+        )
+
+    def halo_goes(l):
+        return s < last if l else inner
+
+    def over(h, body):
+        first, count = parts[h]
+
+        def step(c, carry):
+            body(pl.multiple_of(first + c * CHUNK, CHUNK))
+            return carry
+
+        lax.fori_loop(0, count // CHUNK, step, 0)
+
+    def scale(which, l, source, b, h, fresh):
+        cut = pl.ds(pl.multiple_of(b * part, 128), part)
+
+        def body(low):
+            at = pl.ds(low, CHUNK)
+            x = source[b, at, :].astype(F32)
+            square = x * x
+            total = square[:, 0:128]
+            for j in range(1, part // 128):
+                total = total + square[:, j * 128 : (j + 1) * 128]
+            squares[which, at, :] = total if fresh else squares[which, at, :] + total
+            scaled[which, b, at, :] = (x * gain[l : l + 1, cut].astype(F32)).astype(BF16)
+
+        over(h, body)
+
+    def accumulate(which, l, b, h, fresh):
+        at = rows_of(h)
+        for k, acc in ((SIG, acc_sig), (GATE, acc_gate)):
+            w = banks[k][l, b].reshape(part, local)
+            more = jnp.dot(scaled[which, b, at, :], w, preferred_element_type=F32)
+            acc[which, at, :] = more if fresh else acc[which, at, :] + more
+
+    def blend(which, h):
+        def body(low):
+            at = pl.ds(low, CHUNK)
+            total = jnp.sum(squares[which, at, :], axis=1, keepdims=True)
+            r = lax.rsqrt(total / width + EPS)
+            v = (acc_sig[which, at, :] * r) * sigmoid(acc_gate[which, at, :] * r)
+            v = v.astype(BF16)
+            if which:
+                back[at, :] = v
+            else:
+                padded[pl.ds(pl.multiple_of(hp + low, 8), CHUNK), :] = v.astype(F32)
+
+        over(h, body)
+
+    def send_tail(l):
+        tail[l] = padded[rows : rows + hp, :].astype(BF16)
+
+        @pl.when(halo_goes(l))
+        def _():
+            halo_copy(l).start()
+
+    def settle(l):
+        @pl.when(s >= middle if l == 0 else s > 0)
+        def _():
+            halo_copy(l).wait_recv()
+            padded[0:hp, :] = halo[l].astype(F32)
+
+        if l == 0:
+            @pl.when(inner & (s < middle))
+            def _():
+                padded[0:hp, :] = back[rows - hp : rows, :].astype(F32)
+
+        @pl.when(s == 0)
+        def _():
+            padded[0:hp, :] = jnp.zeros((hp, local), F32)
+
+    def convolve(l, h):
+        begin, count = parts[h]
+        tap_rows = taps[:, l, :].astype(F32)
+        first = hp - (kernel_taps - 1)
+        lane = lax.broadcasted_iota(jnp.int32, (CHUNK, 128), 1)
+        chunks = list(range(begin // CHUNK, (begin + count) // CHUNK))
+        if chunks[0] == 0:
+            chunks = chunks[1:] + chunks[:1]
+        for c in chunks:
+            if c == 0:
+                settle(l)
+            low = c * CHUNK
+            total = jnp.broadcast_to(bias[l : l + 1, :].astype(F32), (CHUNK, local))
+            for j in range(kernel_taps):
+                start = low + first + j
+                total = total + tap_rows[j : j + 1, :] * padded[start : start + CHUNK, :]
+            filt[low : low + CHUNK, :] = total
+            one = jnp.sum(total, axis=1, keepdims=True)
+            two = jnp.sum(total * total, axis=1, keepdims=True)
+            stat_cols[low : low + CHUNK, :] = jnp.where(
+                lane == 0, one, jnp.where(lane == 1, two, 0.0)
+            )
+        at = slice(begin, begin + count)
+        stat_rows[l, t, :, at] = jnp.transpose(stat_cols[at, :])[0:8, :]
+        for i in range(1, tp):
+            stat_copy(l, h, i, t).start()
+
+    def activate(l, h):
+        begin, count = parts[h]
+        at = slice(begin, begin + count)
+        for i in range(1, tp):
+            stat_copy(l, h, i, lax.rem(t + i, tp)).wait_recv()
+        sums = stat_rows[l, 0, :, at]
+        for b in range(1, tp):
+            sums = sums + stat_rows[l, b, :, at]
+        stat_cols[at, :] = jnp.transpose(
+            jnp.concatenate([sums, jnp.zeros((120, count), F32)], axis=0)
+        )
+        gains, shifts = ln_gain[l : l + 1, :].astype(F32), ln_shift[l : l + 1, :].astype(F32)
+
+        def body(low):
+            at = pl.ds(low, CHUNK)
+            average = stat_cols[at, 0:1] / channels
+            spread = stat_cols[at, 1:2] / channels - average * average
+            v = (filt[at, :] - average) * lax.rsqrt(spread + EPS) * gains + shifts
+            acts[l, t, at, :] = (v * sigmoid(v)).astype(BF16)
+
+        over(h, body)
+        spread_start(acts.at[l], layers + l, h)
+
+    def update(l, h):
+        begin, count = parts[h]
+        tile = min(256, part)
+        deep = 128
+
+        def body(c, carry):
+            at = pl.ds(pl.multiple_of(begin + c * deep, deep), deep)
+            for n in range(part // tile):
+                cut = slice(n * tile, (n + 1) * tile)
+                total = feats[l, t, at, cut].astype(F32)
+                for b in range(tp):
+                    w = out_all[l, b, :, :, :, cut].reshape(local, tile)
+                    total = total + jnp.dot(acts[l, b, at, :], w, preferred_element_type=F32)
+                if l + 1 < layers:
+                    feats[l + 1, t, at, cut] = total.astype(BF16)
+                else:
+                    result[at, cut] = total.astype(BF16)
+            return carry
+
+        lax.fori_loop(0, count // deep, body, 0)
+
+    far_n = 2 * layers
+    both_in = (SIG, GATE)
+
+    @pl.when(outer)
+    def _():
+        own_stream.wait()
+        for k in range(3):
+            load(0, k).wait()
+        each(0, (SIG,), lift)
+        far_copy(0).start()
+        each(0, (GATE,), lift)
+        far_copy(1).start()
+        each(0, both_in, lift_other)
+        each(0, (OUT,), lift)
+        each(0, (OUT,), lift_other)
+        for l in range(1, layers):
+            for k in range(3):
+                load(l, k).wait()
+            each(l, range(3), lift)
+        for l in range(1, layers):
+            each(l, range(3), lift_other)
+        each(0, (OUT,), take(mid, False))
+        for l in range(1, layers):
+            each(l, range(3), take(mid, False))
+        each(0, (OUT,), take(mid2, False))
+        for h in both:
+            back_copy(h).wait_recv()
+
+            def body(low):
+                to = pl.ds(pl.multiple_of(hp + low, 8), CHUNK)
+                padded[to, :] = back[pl.ds(low, CHUNK), :].astype(F32)
+
+            over(h, body)
+
+    @pl.when(inner)
+    def _():
+        load(0, SIG).wait()
+        load(0, GATE).wait()
+        each(0, both_in, lambda l, k, q: to_middle(l, k, q, s))
+        own_stream.wait()
+        for h in both:
+            spread_start(feats.at[0], 0, h)
+        load(0, OUT).wait()
+        each(0, (OUT,), onward(s))
+        for l in range(1, layers):
+            for k in range(3):
+                load(l, k).wait()
+            each(l, range(3), onward(s))
+        for q in range(pieces[SIG]):
+            pass_on(0, SIG, q)
+            take(mid2, False)(0, SIG, q)
+        each(0, (GATE,), take(mid2, False))
+        spread_relay(feats.at[0], 0, 0)
+        each(0, (SIG,), take(end2, False))
+        far_copy(0).wait_recv()
+        spread_start(far, far_n, 0)
+        spread_relay(feats.at[0], 0, 1)
+        each(0, (GATE,), pass_on)
+        each(0, (OUT,), lambda l, k, q: to_middle(l, k, q, s))
+        each(1, both_in, lambda l, k, q: to_middle(l, k, q, s))
+        for h in both:
+            spread_near(feats.at[0], 0, h)
+            spread_rest(feats.at[0], 0, h)
+        for h in both:
+            for i, b in enumerate(near_blocks + far_blocks):
+                scale(0, 0, feats.at[0], b, h, i == 0)
+        each(0, (GATE,), take(end2, False))
+        for h in both:
+            accumulate(0, 0, s, h, True)
+        for k in both_in:
+            ready(0, k, mid2)
+        for h in both:
+            accumulate(0, 0, mid2, h, False)
+        far_copy(1).wait_recv()
+        spread_start(far, far_n, 1)
+        each(0, (OUT,), take(mid2))
+        for h in both:
+            spread_relay(far, far_n, h)
+            spread_near(far, far_n, h)
+            spread_rest(far, far_n, h)
+            for i, b in enumerate(near_blocks + far_blocks):
+                scale(1, 0, far, b, h, i == 0)
+            if h == 0:
+                for k in both_in:
+                    ready(0, k, end2)
+                    ready(0, k, end)
+            for i, b in enumerate((s, mid2, end2, end)):
+                accumulate(1, 0, b, h, i == 0)
+            blend(1, h)
+            back_copy(h).start()
+            if h == 0:
+                each(1, (SIG,), take(mid2))
+        for h in both:
+            for b in (end2, end):
+                accumulate(0, 0, b, h, False)
+            blend(0, h)
+            if h == 0:
+                send_tail(0)
+        each(0, (OUT,), pass_on)
+        each(1, (GATE,), take(mid2, False))
+
+    for h in both:
+        convolve(0, h)
+
+    @pl.when(inner)
+    def _():
+        each(0, (OUT,), take(end2))
+        each(1, (GATE,), onward(mid2))
+
+    activate(0, 0)
+
+    @pl.when(inner)
+    def _():
+        each(1, (SIG,), pass_on)
+        each(1, (OUT,), lambda l, k, q: to_middle(l, k, q, s))
+
+    @pl.when(outer)
+    def _():
+        each(0, (OUT,), take(end2, False))
+        each(1, (SIG,), take(mid2, False))
+
+    activate(0, 1)
+    for h in both:
+        spread_relay(acts.at[0], layers, h)
+    ready_all(0, OUT)
+    for h in both:
+        spread_near(acts.at[0], layers, h)
+        spread_rest(acts.at[0], layers, h)
+        update(0, h)
+        spread_start(feats.at[1], 1, h)
+
+    for l in range(1, layers):
+        x = feats.at[l]
+        for h in both:
+            scale(0, l, x, t, h, True)
+
+        @pl.when(inner)
+        def _(l=l):
+            each(l, (GATE,), pass_on)
+            each(l, both_in, take(end2))
+            each(l, (OUT,), pass_on)
+            each(l, (OUT,), take(mid2))
+
+        @pl.when(outer)
+        def _(l=l):
+            each(l, (GATE,), take(mid2, False))
+            each(l, both_in, take(end2, False))
+
+        for h in both:
+            spread_near(x, l, h)
+            scale(0, l, x, mate, h, False)
+        for k in both_in:
+            ready_all(l, k)
+        for h in both:
+            for i, b in enumerate(near_blocks):
+                accumulate(0, l, b, h, i == 0)
+        spread_relay(x, l, 0)
+
+        @pl.when(outer)
+        def _(l=l):
+            each(l, (OUT,), take(mid2, False))
+
+        for h in both:
+            if h:
+                spread_relay(x, l, h)
+            spread_rest(x, l, h)
+            for b in far_blocks:
+                scale(0, l, x, b, h, False)
+                accumulate(0, l, b, h, False)
+            blend(0, h)
+            if h == 0:
+                send_tail(l)
+                each_role = (inner, outer)
+                for role, further in zip(each_role, (True, False)):
+                    @pl.when(role)
+                    def _(l=l, further=further):
+                        each(l, (OUT,), take(end2, further))
+        for h in both:
+            convolve(l, h)
+        for h in both:
+            activate(l, h)
+        for h in both:
+            spread_relay(acts.at[l], layers + l, h)
+        ready_all(l, OUT)
+        for h in both:
+            spread_near(acts.at[l], layers + l, h)
+            spread_rest(acts.at[l], layers + l, h)
+            update(l, h)
+            if l + 1 < layers:
+                spread_start(feats.at[l + 1], l + 1, h)
+
+    @pl.when(outer)
+    def _():
+        for h in both:
+            far_copy(h).wait_send()
+        for l in range(layers):
+            each(l, range(3), lambda l, k, q: lift(l, k, q, True))
+            each(l, range(3), lambda l, k, q: lift_other(l, k, q, True))
+            for shard in (mid, mid2, end2):
+                each(l, range(3) if l else (OUT,), lambda l, k, q: across(l, k, q, shard, True))
+
+    @pl.when(inner)
+    def _():
+        spread_done(feats.at[0], 0)
+        spread_done(far, far_n)
+        for h in both:
+            back_copy(h).wait_send()
+        for l in range(layers):
+            for shard in (s, end):
+                each(l, range(3), lambda l, k, q: to_middle(l, k, q, shard, True))
+            for shard in (s, mid2, end2):
+                each(l, range(3) if l else (OUT,), lambda l, k, q: to_end(l, k, q, shard, True))
+            for shard in (mid2, end2):
+                each(l, range(3), lambda l, k, q: across(l, k, q, shard, True))
+            for k in range(3):
+                for q in range(pieces[k]):
+                    if not direct(l, k, q, pieces[k]):
+                        across(l, k, q, end, True)
+
+    for l in range(layers):
+        if l:
+            spread_done(feats.at[l], l)
+        spread_done(acts.at[l], layers + l)
+        for h in both:
+            for i in range(1, tp):
+                stat_copy(l, h, i, t).wait_send()
+
+        @pl.when(halo_goes(l))
+        def _(l=l):
+            halo_copy(l).wait_send()
+
+
 def shards(counts, stream, norm_gain, w_signal, w_gate, conv_taps, conv_bias, ln_gain, ln_shift, w_out):
     groups, sp, tp = counts
     layers, deep, local = w_signal.shape
@@ -392,14 +976,35 @@
     dma = lambda *shape: pltpu.SemaphoreType.DMA(shape)
     anywhere = pl.BlockSpec(memory_space=pl.ANY)
     inside = pl.BlockSpec(memory_space=pltpu.VMEM)
-    return pl.pallas_call(
-        functools.partial(
-            kernel, (groups, sp, tp, layers, rows, kernel_taps, hp, width, channels)
-        ),
-        out_shape=jax.ShapeDtypeStruct(stream.shape, BF16),
-        in_specs=[anywhere, inside, anywhere, anywhere, inside, inside, inside, inside, anywhere],
-        out_specs=inside,
-        scratch_shapes=[
+    spreads = (2 * layers + 1, 2, tp)
+    folds = groups == 2 and layers == 2 and sp == tp and sp // 2 == 2 and rows % 128 == 0 and rows > 128
+    if folds:
+        body = fold_kernel
+        scratch = [
+            bank(w_signal), bank(w_gate), bank(w_out),
+            pltpu.VMEM((layers, tp, rows, part), BF16),
+            pltpu.VMEM((tp, rows, part), BF16),
+            pltpu.VMEM((2, tp, rows, part), BF16),
+            pltpu.VMEM((2, rows, 128), F32),
+            pltpu.VMEM((2, rows, local), F32),
+            pltpu.VMEM((2, rows, local), F32),
+            pltpu.VMEM((rows, local), BF16),
+            pltpu.VMEM((layers, hp, local), BF16),
+            pltpu.VMEM((layers, hp, local), BF16),
+            pltpu.VMEM((hp + rows, local), F32),
+            pltpu.VMEM((rows, local), F32),
+            pltpu.VMEM((rows, 128), F32),
+            pltpu.VMEM((layers, tp, 8, rows), F32),
+            pltpu.VMEM((layers, tp, rows, local), BF16),
+            dma(layers, 3), pltpu.SemaphoreType.DMA,
+            dma(*line), dma(*line), dma(*line), dma(*line), dma(*line),
+            dma(*spreads), dma(*spreads), dma(*spreads), dma(*spreads),
+            dma(2), dma(2), dma(2), dma(2),
+            dma(layers), dma(layers), dma(layers, 2, tp), dma(layers, 2, tp),
+        ]
+    else:
+        body = kernel
+        scratch = [
             bank(w_signal), bank(w_gate), bank(w_out),
             pltpu.VMEM((layers, tp, rows, part), BF16),
             pltpu.VMEM((tp, rows, part), BF16),
@@ -417,7 +1022,15 @@
             dma(layers, 3, most), dma(*line), dma(*line), dma(*line), dma(*line),
             dma(2 * layers, tp), dma(2 * layers, tp), dma(2 * layers, tp), dma(2 * layers, tp),
             dma(layers), dma(layers), dma(layers, tp), dma(layers, tp),
-        ],
+        ]
+    return pl.pallas_call(
+        functools.partial(
+            body, (groups, sp, tp, layers, rows, kernel_taps, hp, width, channels)
+        ),
+        out_shape=jax.ShapeDtypeStruct(stream.shape, BF16),
+        in_specs=[anywhere, inside, anywhere, anywhere, inside, inside, inside, inside, anywhere],
+        out_specs=inside,
+        scratch_shapes=scratch,
         compiler_params=pltpu.CompilerParams(
             collective_id=0, has_side_effects=True, vmem_limit_bytes=60 * 1024 * 1024
         ),

time: 136 us -> 122 us (0.90)
  Pallas kernels: 133 us -> 119 us
    pallas_call x1, Pallas kernels: 133 us -> 119 us  [shards(): pl.pallas_call(functools.partial(body, (groups, sp, tp, layers, rows, ker...]
where the time goes in v1:
time: 122 us; the launch traced here: 121 us
  Pallas kernels  119 us (98%)
  local copies, waits for them, and re-layouts  2.06 us (2%)
    pallas_call x1, Pallas kernels, shards(): pl.pallas_call(functools.partial(body, (groups, sp, tp, layers, rows, ker...  119 us

profile of v1, /device:TPU:0, one launch (start us, length us, event | category | flops | bytes accessed | tf_op | source)
XLA Modules:
  0.0 121.4 jit_solution(18086317532518076947)
XLA Ops:
  0.0 119.3 %shard_map.91 = bf16[384,1024]{1,0:T(8,128)(2,1)} custom-call(bf16[384,1024]{1,0:T(8,128)(2,1)} %stream.1, bf16[2,4096]{1,0:T(2,128)(2,1)} %gain.1, bf16[2,2,2,256,256]{4,3,2,1,0:T(8,128)(2,1)} %bitcast.4, bf16[2,2,2,256,256]{4,3,2,1,0:T(8,128)(2,1)} %bitcast.5, bf16[31,2,256]{2,1,0:T(2,128)(2,1)} %bitcast.7, bf16[2,256]{1,0:T(2,128)(2,1)} %bias.1, ...), custom_call_target="tpu_custom_call" | custom-call | tf_op jit(solution)/shard_map/pallas_call | solution.py:1026
  119.3 2.1 %copy.11 = bf16[384,1024]{1,0:T(8,128)(2,1)} copy(bf16[384,1024]{1,0:T(8,128)(2,1)} %shard_map.91) | data formatting | bytes 1572864

commit v2 on v1

--- a/solution.py
+++ b/solution.py
@@ -14,6 +14,9 @@
 SIG, GATE, OUT = 0, 1, 2
 CHUNK = 32
 PIECES = 2
+FOLD_PIECES = 4
+DEEP = 128
+PAIR, FAR_MID, FAR_END, OWN = 0, 1, 2, 3
 
 
 def sigmoid(v):
@@ -373,7 +376,7 @@
 
 
 def direct(l, k, q, count):
-    return l > 0 or k == OUT or q < count - 1 or count == 1
+    return l > 0 or k == OUT or q < count // 2 or count == 1
 
 
 def fold_kernel(
@@ -382,7 +385,7 @@
     result,
     sig_all, gate_all, out_all, feats, far, scaled, squares, acc_sig, acc_gate,
     back, tail, halo, padded, filt, stat_cols, stat_rows, acts,
-    load_sem, stream_sem, z_send, end_send, z_recv, y_send, y_recv,
+    final, load_sem, stream_sem, final_sem, z_send, end_send, z_recv, y_send, y_recv,
     cross_send, cross_recv, core_send, core_recv,
     far_send, far_recv, back_send, back_recv,
     halo_send, halo_recv, stat_send, stat_recv,
@@ -403,8 +406,8 @@
     held = (w_signal, w_gate, w_out)
     pieces = [w.shape[2] for w in held]
     local, part = channels // tp, width // tp
-    parts = ((128, rows - 128), (0, 128))
-    both = range(len(parts))
+    parts = [(rows - (h + 1) * DEEP, DEEP) for h in range(rows // DEEP)]
+    every = range(len(parts))
     other_group = {"grp": 1 - g}
 
     def load(l, k):
@@ -438,73 +441,87 @@
         jnp.where(s > 0, 1, 0) + jnp.where(s < last, 1, 0) + (groups - 1 + tp - 1),
     )
 
-    def z_copy(l, k, q, shard, to, sems):
-        ref = banks[k].at[l, shard, g, q]
+    where = (pair, mid2, end2, s)
+
+    def z_copy(l, k, q, kind, to, sems, spot):
+        ref = banks[k].at[l, where[kind], g, q]
         return pltpu.make_async_remote_copy(
             src_ref=ref, dst_ref=ref,
-            send_sem=sems.at[l, k, q, shard], recv_sem=z_recv.at[l, k, q, shard],
+            send_sem=sems.at[l, k, spot], recv_sem=z_recv.at[l, k, q, spot],
             device_id={"sp": to}, device_id_type=MESH,
         )
 
-    def y_copy(l, k, q, shard, half, where):
-        ref = banks[k].at[l, shard, half, q]
+    def y_copy(l, k, q, kind, half, to, sems, spot):
+        ref = banks[k].at[l, where[kind], half, q]
         return pltpu.make_async_remote_copy(
             src_ref=ref, dst_ref=ref,
-            send_sem=y_send.at[l, k, q, shard], recv_sem=y_recv.at[l, k, q, shard],
-            device_id=where, device_id_type=MESH,
-        )
-
-    def flow(copy, done):
-        copy.wait_send() if done else copy.start()
-
-    def across(l, k, q, shard, done=False):
-        flow(y_copy(l, k, q, shard, g, other_group), done)
-
-    def to_end(l, k, q, shard, done=False):
-        flow(z_copy(l, k, q, shard, end, end_send), done)
-
-    def to_middle(l, k, q, shard, done=False):
-        flow(z_copy(l, k, q, shard, mid2, z_send), done)
-
-    def lift(l, k, q, done=False):
-        flow(z_copy(l, k, q, s, mid, z_send), done)
-
-    def lift_other(l, k, q, done=False):
+            send_sem=sems.at[l, k, spot], recv_sem=y_recv.at[l, k, spot],
+            device_id=to, device_id_type=MESH,
+        )
+
+    def across(l, k, q, kind):
+        y_copy(l, k, q, kind, g, other_group, y_send, kind).start()
+
+    def to_end(l, k, q, kind):
+        z_copy(l, k, q, kind, end, end_send, PAIR if kind == OWN else kind).start()
+
+    def to_middle(l, k, q, kind):
+        z_copy(l, k, q, kind, mid2, z_send, FAR_MID if kind == OWN else FAR_END).start()
+
+    def lift(l, k, q):
+        z_copy(l, k, q, OWN, mid, z_send, PAIR).start()
+
+    def lift_other(l, k, q):
         if direct(l, k, q, pieces[k]):
-            flow(y_copy(l, k, q, s, 1 - g, {"sp": mid}), done)
-
-    def arrived(l, k, q, shard):
-        z_copy(l, k, q, shard, mid, z_send).wait_recv()
-
-    def each(l, kinds, act):
+            y_copy(l, k, q, OWN, 1 - g, {"sp": mid}, end_send, PAIR).start()
+
+    def arrived(l, k, q, kind):
+        z_copy(l, k, q, kind, mid, z_send, kind).wait_recv()
+
+    def each(l, kinds, act, low=0, high=4):
         for k in kinds:
-            for q in range(pieces[k]):
+            for q in range(pieces[k] * low // 4, pieces[k] * high // 4):
                 act(l, k, q)
 
     def pass_on(l, k, q):
-        arrived(l, k, q, end)
-        to_middle(l, k, q, end)
+        arrived(l, k, q, PAIR)
+        to_middle(l, k, q, PAIR)
+
+    def take(kind, onward=True):
+        def act(l, k, q):
+            arrived(l, k, q, kind)
+            across(l, k, q, kind)
+            if onward:
+                to_end(l, k, q, kind)
+        return act
+
+    def onward(kind):
+        return lambda l, k, q: to_end(l, k, q, kind)
+
+    def bypass(kind):
+        return lambda l, k, q: across(l, k, q, kind)
+
+    def share_rest(l, k, q):
         if not direct(l, k, q, pieces[k]):
-            across(l, k, q, end)
-
-    def take(shard, onward=True):
-        def act(l, k, q):
-            arrived(l, k, q, shard)
-            across(l, k, q, shard)
-            if onward:
-                to_end(l, k, q, shard)
-        return act
-
-    def onward(shard):
-        return lambda l, k, q: to_end(l, k, q, shard)
-
-    def ready(l, k, shard):
-        for q in range(pieces[k]):
-            y_copy(l, k, q, shard, 1 - g, other_group).wait_recv()
+            across(l, k, q, PAIR)
+
+    def got(kind):
+        return lambda l, k, q: arrived(l, k, q, kind)
+
+    def own_in(l, k, q):
+        to_middle(l, k, q, OWN)
+
+    def ready(l, k, kind):
+        ref = banks[k].at[l, where[kind], 1 - g]
+        pltpu.make_async_copy(ref, ref, y_recv.at[l, k, kind]).wait()
 
     def ready_all(l, k):
-        for shard in (pair, mid2, end2):
-            ready(l, k, shard)
+        for kind in (PAIR, FAR_MID, FAR_END):
+            ready(l, k, kind)
+
+    def sent(l, k, sems, spot, low=0):
+        ref = banks[k].at[l, s, g, pl.ds(low, pieces[k] - low)]
+        pltpu.make_async_copy(ref, ref, sems.at[l, k, spot]).wait()
 
     def rows_of(h):
         return pl.ds(parts[h][0], parts[h][1])
@@ -513,42 +530,45 @@
         ref = buf.at[block, rows_of(h)]
         return pltpu.make_async_remote_copy(
             src_ref=ref, dst_ref=ref,
-            send_sem=cross_send.at[n, h, i], recv_sem=cross_recv.at[n, h, block],
+            send_sem=cross_send.at[n, i - 1], recv_sem=cross_recv.at[n, h, i - 1],
             device_id={"tp": lax.rem(chip + i, chips) * 2 + core}, device_id_type=MESH,
         )
 
-    def core_copy(buf, n, h, block):
+    def core_copy(buf, n, h, block, i):
         ref = buf.at[block, rows_of(h)]
         return pltpu.make_async_remote_copy(
             src_ref=ref, dst_ref=ref,
-            send_sem=core_send.at[n, h, block], recv_sem=core_recv.at[n, h, block],
+            send_sem=core_send.at[n, i], recv_sem=core_recv.at[n, h, i],
             device_id={"tp": mate}, device_id_type=MESH,
         )
+
+    def chip_at(i):
+        return lax.rem(chip + i, chips) * 2
 
     def spread_start(buf, n, h):
         for i in range(1, chips):
             cross_copy(buf, n, h, t, i).start()
-        core_copy(buf, n, h, t).start()
+        core_copy(buf, n, h, t, 0).start()
 
     def spread_relay(buf, n, h):
         for i in range(1, chips):
-            block = lax.rem(chip + i, chips) * 2 + core
-            cross_copy(buf, n, h, block, i).wait_recv()
-            core_copy(buf, n, h, block).start()
+            block = chip_at(i) + core
+            cross_copy(buf, n, h, block, chips - i).wait_recv()
+            core_copy(buf, n, h, block, i).start()
 
     def spread_near(buf, n, h):
-        core_copy(buf, n, h, mate).wait_recv()
+        core_copy(buf, n, h, mate, 0).wait_recv()
 
     def spread_rest(buf, n, h):
         for i in range(1, chips):
-            core_copy(buf, n, h, lax.rem(chip + i, chips) * 2 + 1 - core).wait_recv()
+            core_copy(buf, n, h, chip_at(i) + 1 - core, i).wait_recv()
 
     def spread_done(buf, n):
-        for h in both:
-            for i in range(1, chips):
-                cross_copy(buf, n, h, t, i).wait_send()
-            for j in range(chips):
-                core_copy(buf, n, h, j * 2 + core).wait_send()
+        ref = buf.at[t]
+        for i in range(1, chips):
+            pltpu.make_async_copy(ref, ref, cross_send.at[n, i - 1]).wait()
+        for i in range(chips):
+            pltpu.make_async_copy(ref, ref, core_send.at[n, i]).wait()
 
     far_blocks = [lax.rem(chip + i, chips) * 2 + c for i in range(1, chips) for c in (core, 1 - core)]
     near_blocks = [t, mate]
@@ -556,7 +576,7 @@
     def far_copy(h):
         return pltpu.make_async_remote_copy(
             src_ref=feats.at[0, t, rows_of(h)], dst_ref=far.at[t, rows_of(h)],
-            send_sem=far_send.at[h], recv_sem=far_recv.at[h],
+            send_sem=far_send, recv_sem=far_recv.at[h],
             device_id={"sp": mid}, device_id_type=MESH,
         )
 
@@ -564,7 +584,7 @@
         ref = back.at[rows_of(h)]
         return pltpu.make_async_remote_copy(
             src_ref=ref, dst_ref=ref,
-            send_sem=back_send.at[h], recv_sem=back_recv.at[h],
+            send_sem=back_send, recv_sem=back_recv.at[h],
             device_id={"sp": end}, device_id_type=MESH,
         )
 
@@ -572,7 +592,7 @@
         ref = stat_rows.at[l, block, :, rows_of(h)]
         return pltpu.make_async_remote_copy(
             src_ref=ref, dst_ref=ref,
-            send_sem=stat_send.at[l, h, i], recv_sem=stat_recv.at[l, h, block],
+            send_sem=stat_send.at[l, i - 1], recv_sem=stat_recv.at[l, h],
             device_id={"tp": lax.rem(t + i, tp)}, device_id_type=MESH,
         )
 
@@ -683,8 +703,8 @@
     def activate(l, h):
         begin, count = parts[h]
         at = slice(begin, begin + count)
-        for i in range(1, tp):
-            stat_copy(l, h, i, lax.rem(t + i, tp)).wait_recv()
+        ref = stat_rows.at[l, pl.ds(0, tp - 1), :, rows_of(h)]
+        pltpu.make_async_copy(ref, ref, stat_recv.at[l, h]).wait()
         sums = stat_rows[l, 0, :, at]
         for b in range(1, tp):
             sums = sums + stat_rows[l, b, :, at]
@@ -703,13 +723,17 @@
         over(h, body)
         spread_start(acts.at[l], layers + l, h)
 
+    def write(h):
+        return pltpu.make_async_copy(
+            final.at[rows_of(h)], result.at[rows_of(h)], final_sem
+        )
+
     def update(l, h):
         begin, count = parts[h]
         tile = min(256, part)
-        deep = 128
 
         def body(c, carry):
-            at = pl.ds(pl.multiple_of(begin + c * deep, deep), deep)
+            at = pl.ds(pl.multiple_of(begin + c * DEEP, DEEP), DEEP)
             for n in range(part // tile):
                 cut = slice(n * tile, (n + 1) * tile)
                 total = feats[l, t, at, cut].astype(F32)
@@ -719,241 +743,308 @@
                 if l + 1 < layers:
                     feats[l + 1, t, at, cut] = total.astype(BF16)
                 else:
-                    result[at, cut] = total.astype(BF16)
+                    final[at, cut] = total.astype(BF16)
             return carry
 
-        lax.fori_loop(0, count // deep, body, 0)
+        lax.fori_loop(0, count // DEEP, body, 0)
+        if l + 1 == layers:
+            write(h).start()
 
     far_n = 2 * layers
     both_in = (SIG, GATE)
+
+    def spread_end(buf, n, h):
+        spread_relay(buf, n, h)
+        spread_near(buf, n, h)
+        spread_rest(buf, n, h)
+
+    def scale_all(which, l, source, h):
+        for i, b in enumerate(near_blocks + far_blocks):
+            scale(which, l, source, b, h, i == 0)
+
+    def fetch(h):
+        back_copy(h).wait_recv()
+
+        def body(low):
+            to = pl.ds(pl.multiple_of(hp + low, 8), CHUNK)
+            padded[to, :] = back[pl.ds(low, CHUNK), :].astype(F32)
+
+        over(h, body)
+
+    def settle_far(h, blocks):
+        for i, b in enumerate(blocks):
+            accumulate(1, 0, b, h, i == 0)
+        blend(1, h)
+        back_copy(h).start()
 
     @pl.when(outer)
     def _():
         own_stream.wait()
         for k in range(3):
             load(0, k).wait()
-        each(0, (SIG,), lift)
-        far_copy(0).start()
-        each(0, (GATE,), lift)
-        far_copy(1).start()
+        each(0, both_in, lift)
+        for h in every:
+            far_copy(h).start()
         each(0, both_in, lift_other)
         each(0, (OUT,), lift)
+        for k in range(3):
+            load(1, k).wait()
+        each(1, (SIG,), lift)
         each(0, (OUT,), lift_other)
-        for l in range(1, layers):
-            for k in range(3):
-                load(l, k).wait()
-            each(l, range(3), lift)
-        for l in range(1, layers):
-            each(l, range(3), lift_other)
-        each(0, (OUT,), take(mid, False))
-        for l in range(1, layers):
-            each(l, range(3), take(mid, False))
-        each(0, (OUT,), take(mid2, False))
-        for h in both:
-            back_copy(h).wait_recv()
-
-            def body(low):
-                to = pl.ds(pl.multiple_of(hp + low, 8), CHUNK)
-                padded[to, :] = back[pl.ds(low, CHUNK), :].astype(F32)
-
-            over(h, body)
+        each(1, (GATE, OUT), lift)
+        each(1, range(3), lift_other)
+        each(0, (OUT,), take(PAIR, False))
+        each(1, range(3), take(PAIR, False))
+        each(0, (OUT,), take(FAR_MID, False))
+        each(1, (SIG,), take(FAR_MID, False), 0, 3)
+        fetch(0)
 
     @pl.when(inner)
     def _():
         load(0, SIG).wait()
         load(0, GATE).wait()
-        each(0, both_in, lambda l, k, q: to_middle(l, k, q, s))
+        each(0, both_in, own_in)
         own_stream.wait()
-        for h in both:
+        for h in every:
             spread_start(feats.at[0], 0, h)
         load(0, OUT).wait()
-        each(0, (OUT,), onward(s))
-        for l in range(1, layers):
-            for k in range(3):
-                load(l, k).wait()
-            each(l, range(3), onward(s))
-        for q in range(pieces[SIG]):
-            pass_on(0, SIG, q)
-            take(mid2, False)(0, SIG, q)
-        each(0, (GATE,), take(mid2, False))
-        spread_relay(feats.at[0], 0, 0)
-        each(0, (SIG,), take(end2, False))
+        each(0, (OUT,), onward(OWN))
+        for k in range(3):
+            load(1, k).wait()
+        each(1, range(3), onward(OWN))
+        for k in both_in:
+            for q in range(pieces[k]):
+                pass_on(0, k, q)
+                take(FAR_MID, False)(0, k, q)
+            spread_relay(feats.at[0], 0, k)
+        each(0, (OUT,), own_in)
+        each(1, both_in, own_in)
+        each(0, (SIG,), take(FAR_END, False))
         far_copy(0).wait_recv()
         spread_start(far, far_n, 0)
-        spread_relay(feats.at[0], 0, 1)
-        each(0, (GATE,), pass_on)
-        each(0, (OUT,), lambda l, k, q: to_middle(l, k, q, s))
-        each(1, both_in, lambda l, k, q: to_middle(l, k, q, s))
-        for h in both:
+        for h in every[2:]:
+            spread_relay(feats.at[0], 0, h)
+        each(0, (GATE,), take(FAR_END, False), 0, 3)
+        for h in every[1:-1]:
+            far_copy(h).wait_recv()
+            spread_start(far, far_n, h)
+        each(0, (GATE,), take(FAR_END, False), 3, 4)
+        each(0, both_in, share_rest)
+        for h in every:
             spread_near(feats.at[0], 0, h)
             spread_rest(feats.at[0], 0, h)
-        for h in both:
-            for i, b in enumerate(near_blocks + far_blocks):
-                scale(0, 0, feats.at[0], b, h, i == 0)
-        each(0, (GATE,), take(end2, False))
-        for h in both:
-            accumulate(0, 0, s, h, True)
+            scale_all(0, 0, feats.at[0], h)
+        spread_end(far, far_n, 0)
+        scale_all(1, 0, far, 0)
+        each(0, (OUT,), got(FAR_MID))
+        each(0, (OUT,), onward(FAR_MID))
+        far_copy(every[-1]).wait_recv()
+        spread_start(far, far_n, every[-1])
+        for h in every[1:-1]:
+            spread_relay(far, far_n, h)
+        each(0, (OUT,), bypass(FAR_MID))
         for k in both_in:
-            ready(0, k, mid2)
-        for h in both:
-            accumulate(0, 0, mid2, h, False)
-        far_copy(1).wait_recv()
-        spread_start(far, far_n, 1)
-        each(0, (OUT,), take(mid2))
-        for h in both:
-            spread_relay(far, far_n, h)
+            ready(0, k, FAR_MID)
+        for h in every:
+            for i, b in enumerate((s, mid2)):
+                accumulate(0, 0, b, h, i == 0)
+        each(1, (SIG,), take(FAR_MID), 0, 3)
+        for h in every[1:-1]:
             spread_near(far, far_n, h)
             spread_rest(far, far_n, h)
-            for i, b in enumerate(near_blocks + far_blocks):
-                scale(1, 0, far, b, h, i == 0)
-            if h == 0:
-                for k in both_in:
-                    ready(0, k, end2)
-                    ready(0, k, end)
-            for i, b in enumerate((s, mid2, end2, end)):
-                accumulate(1, 0, b, h, i == 0)
-            blend(1, h)
-            back_copy(h).start()
-            if h == 0:
-                each(1, (SIG,), take(mid2))
-        for h in both:
+            scale_all(1, 0, far, h)
+        for k in both_in:
+            ready(0, k, FAR_END)
+            ready(0, k, PAIR)
+        blocks = (s, mid2, end2, end)
+        settle_far(0, blocks)
+        each(0, (OUT,), pass_on, 0, 2)
+        for h in every[1:-1]:
+            settle_far(h, blocks)
+        each(0, (OUT,), pass_on, 2, 4)
+        spread_end(far, far_n, every[-1])
+        scale_all(1, 0, far, every[-1])
+        settle_far(every[-1], blocks)
+        each(1, (SIG,), take(FAR_MID), 3, 4)
+        each(1, (GATE,), take(FAR_MID), 0, 2)
+        for h in every:
             for b in (end2, end):
                 accumulate(0, 0, b, h, False)
             blend(0, h)
             if h == 0:
                 send_tail(0)
-        each(0, (OUT,), pass_on)
-        each(1, (GATE,), take(mid2, False))
-
-    for h in both:
+        each(1, (SIG,), pass_on)
+        each(1, (OUT,), own_in)
+        each(1, (GATE,), got(FAR_MID), 2, 4)
+
+    for h in every:
+        if h + 1 < len(parts):
+            @pl.when(outer)
+            def _(h=h):
+                fetch(h + 1)
         convolve(0, h)
 
     @pl.when(inner)
     def _():
-        each(0, (OUT,), take(end2))
-        each(1, (GATE,), onward(mid2))
-
-    activate(0, 0)
+        each(0, (OUT,), take(FAR_END))
+        each(1, (GATE,), bypass(FAR_MID), 2, 4)
+        each(1, (GATE,), onward(FAR_MID), 2, 4)
+
+    @pl.when(outer)
+    def _():
+        each(1, (SIG,), take(FAR_MID, False), 3, 4)
+        each(1, (GATE,), take(FAR_MID, False), 0, 2)
+
+    for h in every:
+        activate(0, h)
+        if h == 0:
+            @pl.when(outer)
+            def _():
+                each(0, (OUT,), take(FAR_END, False))
 
     @pl.when(inner)
     def _():
-        each(1, (SIG,), pass_on)
-        each(1, (OUT,), lambda l, k, q: to_middle(l, k, q, s))
-
-    @pl.when(outer)
-    def _():
-        each(0, (OUT,), take(end2, False))
-        each(1, (SIG,), take(mid2, False))
-
-    activate(0, 1)
-    for h in both:
+        each(1, (SIG,), take(FAR_END))
+
+    for h in every:
         spread_relay(acts.at[0], layers, h)
-    ready_all(0, OUT)
-    for h in both:
+        if h == 0:
+            ready_all(0, OUT)
         spread_near(acts.at[0], layers, h)
         spread_rest(acts.at[0], layers, h)
         update(0, h)
         spread_start(feats.at[1], 1, h)
 
-    for l in range(1, layers):
-        x = feats.at[l]
-        for h in both:
-            scale(0, l, x, t, h, True)
-
         @pl.when(inner)
-        def _(l=l):
-            each(l, (GATE,), pass_on)
-            each(l, both_in, take(end2))
-            each(l, (OUT,), pass_on)
-            each(l, (OUT,), take(mid2))
+        def _(h=h):
+            each(1, (GATE,), pass_on, 2 * h, min(2 * h + 2, 4))
 
         @pl.when(outer)
-        def _(l=l):
-            each(l, (GATE,), take(mid2, False))
-            each(l, both_in, take(end2, False))
-
-        for h in both:
-            spread_near(x, l, h)
-            scale(0, l, x, mate, h, False)
-        for k in both_in:
-            ready_all(l, k)
-        for h in both:
-            for i, b in enumerate(near_blocks):
-                accumulate(0, l, b, h, i == 0)
-        spread_relay(x, l, 0)
-
-        @pl.when(outer)
-        def _(l=l):
-            each(l, (OUT,), take(mid2, False))
-
-        for h in both:
-            if h:
-                spread_relay(x, l, h)
-            spread_rest(x, l, h)
-            for b in far_blocks:
-                scale(0, l, x, b, h, False)
-                accumulate(0, l, b, h, False)
-            blend(0, h)
-            if h == 0:
-                send_tail(l)
-                each_role = (inner, outer)
-                for role, further in zip(each_role, (True, False)):
-                    @pl.when(role)
-                    def _(l=l, further=further):
-                        each(l, (OUT,), take(end2, further))
-        for h in both:
-            convolve(l, h)
-        for h in both:
-            activate(l, h)
-        for h in both:
-            spread_relay(acts.at[l], layers + l, h)
-        ready_all(l, OUT)
-        for h in both:
-            spread_near(acts.at[l], layers + l, h)
-            spread_rest(acts.at[l], layers + l, h)
-            update(l, h)
-            if l + 1 < layers:
-                spread_start(feats.at[l + 1], l + 1, h)
+        def _(h=h):
+            each(1, (GATE,), take(FAR_MID, False), 2 + h, min(3 + h, 4))
+
+    x = feats.at[1]
+    for h in every:
+        scale(0, 1, x, t, h, True)
+
+    @pl.when(inner)
+    def _():
+        each(1, (GATE,), take(FAR_END), 0, 2)
+        each(1, (OUT,), pass_on)
 
     @pl.when(outer)
     def _():
-        for h in both:
-            far_copy(h).wait_send()
+        each(1, (SIG,), take(FAR_END, False))
+
+    for h in every:
+        spread_near(x, 1, h)
+        scale(0, 1, x, mate, h, False)
+
+    @pl.when(inner)
+    def _():
+        each(1, (GATE,), take(FAR_END), 2, 4)
+
+    @pl.when(outer)
+    def _():
+        each(1, (GATE,), take(FAR_END, False), 0, 2)
+
+    spread_relay(x, 1, 0)
+
+    @pl.when(inner)
+    def _():
+        each(1, (OUT,), take(FAR_MID))
+
+    @pl.when(outer)
+    def _():
+        each(1, (GATE,), take(FAR_END, False), 2, 4)
+
+    for k in both_in:
+        ready_all(1, k)
+    for h in every:
+        for i, b in enumerate(near_blocks):
+            accumulate(0, 1, b, h, i == 0)
+    spread_relay(x, 1, 1)
+    for h in every:
+        spread_rest(x, 1, h)
+        for b in far_blocks:
+            scale(0, 1, x, b, h, False)
+            accumulate(0, 1, b, h, False)
+        blend(0, h)
+        if h == 0:
+            send_tail(1)
+
+            @pl.when(inner)
+            def _():
+                each(1, (OUT,), take(FAR_END))
+
+            @pl.when(outer)
+            def _():
+                each(1, (OUT,), take(FAR_MID, False))
+        else:
+            convolve(1, h - 1)
+            if h + 1 < len(parts):
+                spread_relay(x, 1, h + 1)
+    convolve(1, every[-1])
+    activate(1, 0)
+
+    @pl.when(outer)
+    def _():
+        each(1, (OUT,), take(FAR_END, False))
+
+    for h in every[1:]:
+        activate(1, h)
+    spread_relay(acts.at[1], layers + 1, 0)
+    ready_all(1, OUT)
+    for h in every:
+        if h:
+            spread_relay(acts.at[1], layers + 1, h)
+        spread_near(acts.at[1], layers + 1, h)
+        spread_rest(acts.at[1], layers + 1, h)
+        update(1, h)
+
+    @pl.when(outer)
+    def _():
+        pltpu.make_async_copy(feats.at[0, t], feats.at[0, t], far_send).wait()
         for l in range(layers):
-            each(l, range(3), lambda l, k, q: lift(l, k, q, True))
-            each(l, range(3), lambda l, k, q: lift_other(l, k, q, True))
-            for shard in (mid, mid2, end2):
-                each(l, range(3) if l else (OUT,), lambda l, k, q: across(l, k, q, shard, True))
+            for k in range(3):
+                sent(l, k, z_send, PAIR)
+                count = sum(direct(l, k, q, pieces[k]) for q in range(pieces[k]))
+                sent(l, k, end_send, PAIR, pieces[k] - count)
+                if l or k == OUT:
+                    for kind in (PAIR, FAR_MID, FAR_END):
+                        sent(l, k, y_send, kind)
 
     @pl.when(inner)
     def _():
         spread_done(feats.at[0], 0)
         spread_done(far, far_n)
-        for h in both:
-            back_copy(h).wait_send()
+        pltpu.make_async_copy(back, back, back_send).wait()
         for l in range(layers):
-            for shard in (s, end):
-                each(l, range(3), lambda l, k, q: to_middle(l, k, q, shard, True))
-            for shard in (s, mid2, end2):
-                each(l, range(3) if l else (OUT,), lambda l, k, q: to_end(l, k, q, shard, True))
-            for shard in (mid2, end2):
-                each(l, range(3), lambda l, k, q: across(l, k, q, shard, True))
             for k in range(3):
-                for q in range(pieces[k]):
-                    if not direct(l, k, q, pieces[k]):
-                        across(l, k, q, end, True)
+                sent(l, k, z_send, FAR_MID)
+                sent(l, k, z_send, FAR_END)
+                sent(l, k, y_send, FAR_MID)
+                sent(l, k, y_send, FAR_END)
+                if l or k == OUT:
+                    for spot in (PAIR, FAR_MID, FAR_END):
+                        sent(l, k, end_send, spot)
+                count = sum(direct(l, k, q, pieces[k]) for q in range(pieces[k]))
+                if count < pieces[k]:
+                    sent(l, k, y_send, PAIR, count)
 
     for l in range(layers):
         if l:
             spread_done(feats.at[l], l)
         spread_done(acts.at[l], layers + l)
-        for h in both:
-            for i in range(1, tp):
-                stat_copy(l, h, i, t).wait_send()
+        for i in range(1, tp):
+            ref = stat_rows.at[l, t]
+            pltpu.make_async_copy(ref, ref, stat_send.at[l, i - 1]).wait()
 
         @pl.when(halo_goes(l))
         def _(l=l):
             halo_copy(l).wait_send()
+
+    pltpu.make_async_copy(final, final, final_sem).wait()
 
 
 def shards(counts, stream, norm_gain, w_signal, w_gate, conv_taps, conv_bias, ln_gain, ln_shift, w_out):
@@ -964,9 +1055,15 @@
     hp = -(-(kernel_taps - 1) // 16) * 16
     width, channels = part * tp, local * tp
 
+    folds = (
+        groups == 2 and layers == 2 and sp == tp and sp // 2 == 2
+        and rows % DEEP == 0 and rows > DEEP
+    )
+    wanted = FOLD_PIECES if folds else PIECES
+
     def cut(w):
         half = w.shape[1] // groups
-        count = PIECES if half % (16 * PIECES) == 0 else 1
+        count = wanted if half % (16 * wanted) == 0 else 1
         return w.reshape(layers, groups, count, half // count, w.shape[2])
 
     w_signal, w_gate, w_out = cut(w_signal), cut(w_gate), cut(w_out)
@@ -976,8 +1073,8 @@
     dma = lambda *shape: pltpu.SemaphoreType.DMA(shape)
     anywhere = pl.BlockSpec(memory_space=pl.ANY)
     inside = pl.BlockSpec(memory_space=pltpu.VMEM)
-    spreads = (2 * layers + 1, 2, tp)
-    folds = groups == 2 and layers == 2 and sp == tp and sp // 2 == 2 and rows % 128 == 0 and rows > 128
+    count = max(1, rows // DEEP)
+    spreads, chips = 2 * layers + 1, tp // 2
     if folds:
         body = fold_kernel
         scratch = [
@@ -996,11 +1093,14 @@
             pltpu.VMEM((rows, 128), F32),
             pltpu.VMEM((layers, tp, 8, rows), F32),
             pltpu.VMEM((layers, tp, rows, local), BF16),
-            dma(layers, 3), pltpu.SemaphoreType.DMA,
-            dma(*line), dma(*line), dma(*line), dma(*line), dma(*line),
-            dma(*spreads), dma(*spreads), dma(*spreads), dma(*spreads),
-            dma(2), dma(2), dma(2), dma(2),
-            dma(layers), dma(layers), dma(layers, 2, tp), dma(layers, 2, tp),
+            pltpu.VMEM((rows, part), BF16),
+            dma(layers, 3), pltpu.SemaphoreType.DMA, pltpu.SemaphoreType.DMA,
+            dma(layers, 3, 3), dma(layers, 3, 3), dma(layers, 3, most, 3),
+            dma(layers, 3, 3), dma(layers, 3, 3),
+            dma(spreads, chips - 1), dma(spreads, count, chips - 1),
+            dma(spreads, chips), dma(spreads, count, chips),
+            pltpu.SemaphoreType.DMA, dma(count), pltpu.SemaphoreType.DMA, dma(count),
+            dma(layers), dma(layers), dma(layers, tp - 1), dma(layers, count),
         ]
     else:
         body = kernel
@@ -1029,7 +1129,7 @@
         ),
         out_shape=jax.ShapeDtypeStruct(stream.shape, BF16),
         in_specs=[anywhere, inside, anywhere, anywhere, inside, inside, inside, inside, anywhere],
-        out_specs=inside,
+        out_specs=anywhere if folds else inside,
         scratch_shapes=scratch,
         compiler_params=pltpu.CompilerParams(
             collective_id=0, has_side_effects=True, vmem_limit_bytes=60 * 1024 * 1024

time: 122 us -> 111 us (0.910); the launches traced: 121 us -> 109 us
  Pallas kernels: 119 us -> 107 us
    pallas_call x1, Pallas kernels: 119 us -> 107 us  [shards(): pl.pallas_call(functools.partial(body, (groups, sp, tp, layers, rows, ker...]
where the time goes in v2:
time: 111 us; the launch traced here: 109 us
  Pallas kernels  107 us (96%)
  local copies, waits for them, and re-layouts  2.06 us (2%)
    pallas_call x1, Pallas kernels, shards(): pl.pallas_call(functools.partial(body, (groups, sp, tp, layers, rows, ker...  107 us

profile of v2, /device:TPU:0, one launch (start us, length us, event | category | flops | bytes accessed | tf_op | source)
XLA Modules:
  0.0 109.0 jit_solution(14626567320905265977)
XLA Ops:
  0.0 106.9 %shard_map.91 = bf16[384,1024]{1,0:T(8,128)(2,1)} custom-call(bf16[384,1024]{1,0:T(8,128)(2,1)} %stream.1, bf16[2,4096]{1,0:T(2,128)(2,1)} %gain.1, bf16[2,2,4,128,256]{4,3,2,1,0:T(8,128)(2,1)} %bitcast.4, bf16[2,2,4,128,256]{4,3,2,1,0:T(8,128)(2,1)} %bitcast.5, bf16[31,2,256]{2,1,0:T(2,128)(2,1)} %bitcast.7, bf16[2,256]{1,0:T(2,128)(2,1)} %bias.1, ...), custom_call_target="tpu_custom_call" | custom-call | tf_op jit(solution)/shard_map/pallas_call | solution.py:1126
  106.9 2.1 %copy.11 = bf16[384,1024]{1,0:T(8,128)(2,1)} copy(bf16[384,1024]{1,0:T(8,128)(2,1)} %shard_map.91) | data formatting | bytes 1572864

commit v3 on v2

--- a/solution.py
+++ b/solution.py
@@ -376,16 +376,16 @@
 
 
 def direct(l, k, q, count):
-    return l > 0 or k == OUT or q < count // 2 or count == 1
+    return l > 0 or q < count // 2 or count == 1
 
 
 def fold_kernel(
     sizes,
-    stream, gain, w_signal, w_gate, taps, bias, ln_gain, ln_shift, w_out,
-    result,
+    stream, gain_in, w_signal, w_gate, taps_in, bias_in, ln_gain_in, ln_shift_in, w_out,
+    result, gain, taps, bias, ln_gain, ln_shift,
     sig_all, gate_all, out_all, feats, far, scaled, squares, acc_sig, acc_gate,
     back, tail, halo, padded, filt, stat_cols, stat_rows, acts,
-    final, load_sem, stream_sem, final_sem, z_send, end_send, z_recv, y_send, y_recv,
+    final, small_sem, load_sem, stream_sem, final_sem, z_send, end_send, z_recv, y_send, y_recv,
     cross_send, cross_recv, core_send, core_recv,
     far_send, far_recv, back_send, back_recv,
     halo_send, halo_recv, stat_send, stat_recv,
@@ -408,17 +408,20 @@
     local, part = channels // tp, width // tp
     parts = [(rows - (h + 1) * DEEP, DEEP) for h in range(rows // DEEP)]
     every = range(len(parts))
+    both_in = (SIG, GATE)
     other_group = {"grp": 1 - g}
 
     def load(l, k):
         return pltpu.make_async_copy(held[k].at[l], banks[k].at[l, s], load_sem.at[l, k])
 
     own_stream = pltpu.make_async_copy(stream, feats.at[0, t], stream_sem)
-    own_stream.start()
-    for l in range(layers):
-        for k in range(3):
-            load(l, k).start()
-
+    small = [
+        pltpu.make_async_copy(ref, to, small_sem.at[i])
+        for i, (ref, to) in enumerate((
+            (gain_in, gain), (taps_in, taps), (bias_in, bias),
+            (ln_gain_in, ln_gain), (ln_shift_in, ln_shift),
+        ))
+    ]
     barrier = pltpu.get_barrier_semaphore()
 
     def greet(where):
@@ -436,6 +439,15 @@
         greet({"grp": lax.rem(g + i, groups)})
     for i in range(1, tp):
         greet({"tp": lax.rem(t + i, tp)})
+    for k in both_in:
+        load(0, k).start()
+    own_stream.start()
+    load(0, OUT).start()
+    for l in range(1, layers):
+        for k in range(3):
+            load(l, k).start()
+    for copy in small:
+        copy.start()
     pl.semaphore_wait(
         barrier,
         jnp.where(s > 0, 1, 0) + jnp.where(s < last, 1, 0) + (groups - 1 + tp - 1),
@@ -490,9 +502,10 @@
     def take(kind, onward=True):
         def act(l, k, q):
             arrived(l, k, q, kind)
-            across(l, k, q, kind)
             if onward:
                 to_end(l, k, q, kind)
+            if not (onward and kind == FAR_MID and whole(l, k)):
+                across(l, k, q, kind)
         return act
 
     def onward(kind):
@@ -510,6 +523,12 @@
 
     def own_in(l, k, q):
         to_middle(l, k, q, OWN)
+
+    def whole(l, k):
+        return l == layers - 1 and k == OUT
+
+    def own_other(l, k, q):
+        y_copy(l, k, q, OWN, 1 - g, {"sp": mid2}, y_send, FAR_MID).start()
 
     def ready(l, k, kind):
         ref = banks[k].at[l, where[kind], 1 - g]
@@ -630,9 +649,10 @@
 
         over(h, body)
 
-    def accumulate(which, l, b, h, fresh):
+    def accumulate(which, l, b, h, fresh, kinds=(SIG, GATE)):
         at = rows_of(h)
-        for k, acc in ((SIG, acc_sig), (GATE, acc_gate)):
+        for k in kinds:
+            acc = (acc_sig, acc_gate)[k]
             w = banks[k][l, b].reshape(part, local)
             more = jnp.dot(scaled[which, b, at, :], w, preferred_element_type=F32)
             acc[which, at, :] = more if fresh else acc[which, at, :] + more
@@ -673,14 +693,13 @@
         def _():
             padded[0:hp, :] = jnp.zeros((hp, local), F32)
 
-    def convolve(l, h):
+    def convolve(l, h, stages=(0, 1)):
         begin, count = parts[h]
         tap_rows = taps[:, l, :].astype(F32)
         first = hp - (kernel_taps - 1)
         lane = lax.broadcasted_iota(jnp.int32, (CHUNK, 128), 1)
         chunks = list(range(begin // CHUNK, (begin + count) // CHUNK))
-        if chunks[0] == 0:
-            chunks = chunks[1:] + chunks[:1]
+        chunks = (chunks[1:] if 0 in stages else []) + (chunks[:1] if 1 in stages else [])
         for c in chunks:
             if c == 0:
                 settle(l)
@@ -695,6 +714,8 @@
             stat_cols[low : low + CHUNK, :] = jnp.where(
                 lane == 0, one, jnp.where(lane == 1, two, 0.0)
             )
+        if 1 not in stages:
+            return
         at = slice(begin, begin + count)
         stat_rows[l, t, :, at] = jnp.transpose(stat_cols[at, :])[0:8, :]
         for i in range(1, tp):
@@ -751,7 +772,6 @@
             write(h).start()
 
     far_n = 2 * layers
-    both_in = (SIG, GATE)
 
     def spread_end(buf, n, h):
         spread_relay(buf, n, h)
@@ -779,10 +799,11 @@
 
     @pl.when(outer)
     def _():
+        for k in both_in:
+            load(0, k).wait()
+            each(0, (k,), lift)
         own_stream.wait()
-        for k in range(3):
-            load(0, k).wait()
-        each(0, both_in, lift)
+        load(0, OUT).wait()
         for h in every:
             far_copy(h).start()
         each(0, both_in, lift_other)
@@ -791,19 +812,22 @@
             load(1, k).wait()
         each(1, (SIG,), lift)
         each(0, (OUT,), lift_other)
-        each(1, (GATE, OUT), lift)
-        each(1, range(3), lift_other)
+        each(1, (GATE,), lift)
+        each(1, (SIG,), lift_other)
+        each(1, (OUT,), lift)
+        each(1, (GATE, OUT), lift_other)
         each(0, (OUT,), take(PAIR, False))
         each(1, range(3), take(PAIR, False))
         each(0, (OUT,), take(FAR_MID, False))
         each(1, (SIG,), take(FAR_MID, False), 0, 3)
         fetch(0)
+        each(1, (SIG,), take(FAR_MID, False), 3, 4)
 
     @pl.when(inner)
     def _():
-        load(0, SIG).wait()
-        load(0, GATE).wait()
-        each(0, both_in, own_in)
+        for k in both_in:
+            load(0, k).wait()
+            each(0, (k,), own_in)
         own_stream.wait()
         for h in every:
             spread_start(feats.at[0], 0, h)
@@ -818,7 +842,7 @@
                 take(FAR_MID, False)(0, k, q)
             spread_relay(feats.at[0], 0, k)
         each(0, (OUT,), own_in)
-        each(1, both_in, own_in)
+        each(1, (SIG,), own_in)
         each(0, (SIG,), take(FAR_END, False))
         far_copy(0).wait_recv()
         spread_start(far, far_n, 0)
@@ -830,25 +854,29 @@
             spread_start(far, far_n, h)
         each(0, (GATE,), take(FAR_END, False), 3, 4)
         each(0, both_in, share_rest)
+        small[0].wait()
         for h in every:
             spread_near(feats.at[0], 0, h)
             spread_rest(feats.at[0], 0, h)
             scale_all(0, 0, feats.at[0], h)
+            each(0, (OUT,), take(FAR_MID), h, h + 1)
         spread_end(far, far_n, 0)
+        each(0, (OUT,), take(FAR_MID), len(parts), 4)
         scale_all(1, 0, far, 0)
-        each(0, (OUT,), got(FAR_MID))
-        each(0, (OUT,), onward(FAR_MID))
+        for k in both_in:
+            ready(0, k, FAR_MID)
+        for h in every[:1]:
+            for i, b in enumerate((s, mid2)):
+                accumulate(0, 0, b, h, i == 0)
         far_copy(every[-1]).wait_recv()
         spread_start(far, far_n, every[-1])
+        for h in every[1:]:
+            for i, b in enumerate((s, mid2)):
+                accumulate(0, 0, b, h, i == 0)
+        each(1, (SIG,), take(FAR_MID), 0, 1)
         for h in every[1:-1]:
             spread_relay(far, far_n, h)
-        each(0, (OUT,), bypass(FAR_MID))
-        for k in both_in:
-            ready(0, k, FAR_MID)
-        for h in every:
-            for i, b in enumerate((s, mid2)):
-                accumulate(0, 0, b, h, i == 0)
-        each(1, (SIG,), take(FAR_MID), 0, 3)
+        each(1, (SIG,), take(FAR_MID), 1, 3)
         for h in every[1:-1]:
             spread_near(far, far_n, h)
             spread_rest(far, far_n, h)
@@ -858,57 +886,85 @@
             ready(0, k, PAIR)
         blocks = (s, mid2, end2, end)
         settle_far(0, blocks)
-        each(0, (OUT,), pass_on, 0, 2)
+        each(1, (SIG,), take(FAR_MID), 3, 4)
+        each(0, (OUT,), pass_on, 0, 1)
         for h in every[1:-1]:
             settle_far(h, blocks)
-        each(0, (OUT,), pass_on, 2, 4)
+        each(0, (OUT,), pass_on, 1, 3)
         spread_end(far, far_n, every[-1])
         scale_all(1, 0, far, every[-1])
+        each(0, (OUT,), pass_on, 3, 4)
+        each(1, (GATE,), own_in)
         settle_far(every[-1], blocks)
-        each(1, (SIG,), take(FAR_MID), 3, 4)
-        each(1, (GATE,), take(FAR_MID), 0, 2)
+        each(0, (OUT,), share_rest)
+        each(0, (OUT,), take(FAR_END), 0, 1)
         for h in every:
             for b in (end2, end):
                 accumulate(0, 0, b, h, False)
             blend(0, h)
             if h == 0:
                 send_tail(0)
-        each(1, (SIG,), pass_on)
-        each(1, (OUT,), own_in)
-        each(1, (GATE,), got(FAR_MID), 2, 4)
-
+            each(0, (OUT,), take(FAR_END), h + 1, h + 2)
+        each(1, (SIG,), pass_on, 0, 2)
+
+    @pl.when(outer)
+    def _():
+        small[0].wait()
+
+    for copy in small[1:]:
+        copy.wait()
+    convolve(0, 0, (0,))
     for h in every:
         if h + 1 < len(parts):
             @pl.when(outer)
             def _(h=h):
                 fetch(h + 1)
-        convolve(0, h)
+
+        convolve(0, h, (1,))
+        if h + 1 < len(parts):
+            convolve(0, h + 1, (0,))
+
+        @pl.when(outer)
+        def _(h=h):
+            if h:
+                each(0, (OUT,), take(FAR_END, False), h - 1, h)
+
+        if h == 0:
+            @pl.when(inner)
+            def _():
+                each(1, (SIG,), pass_on, 2, 3)
 
     @pl.when(inner)
     def _():
-        each(0, (OUT,), take(FAR_END))
-        each(1, (GATE,), bypass(FAR_MID), 2, 4)
-        each(1, (GATE,), onward(FAR_MID), 2, 4)
-
-    @pl.when(outer)
-    def _():
-        each(1, (SIG,), take(FAR_MID, False), 3, 4)
-        each(1, (GATE,), take(FAR_MID, False), 0, 2)
+        each(1, (SIG,), pass_on, 3, 4)
+        each(1, (GATE,), take(FAR_MID), 0, 2)
 
     for h in every:
         activate(0, h)
         if h == 0:
             @pl.when(outer)
             def _():
-                each(0, (OUT,), take(FAR_END, False))
+                each(0, (OUT,), take(FAR_END, False), 2, 4)
+
+            @pl.when(inner)
+            def _():
+                each(1, (GATE,), take(FAR_MID), 2, 4)
 
     @pl.when(inner)
     def _():
-        each(1, (SIG,), take(FAR_END))
+        each(1, (SIG,), take(FAR_END), 0, 3)
+
+    @pl.when(outer)
+    def _():
+        each(1, (GATE,), take(FAR_MID, False), 0, 2)
 
     for h in every:
         spread_relay(acts.at[0], layers, h)
         if h == 0:
+            @pl.when(outer)
+            def _():
+                each(1, (GATE,), take(FAR_MID, False), 2, 3)
+
             ready_all(0, OUT)
         spread_near(acts.at[0], layers, h)
         spread_rest(acts.at[0], layers, h)
@@ -917,11 +973,16 @@
 
         @pl.when(inner)
         def _(h=h):
+            if h == 0:
+                each(1, (SIG,), take(FAR_END), 3, 4)
             each(1, (GATE,), pass_on, 2 * h, min(2 * h + 2, 4))
 
         @pl.when(outer)
         def _(h=h):
-            each(1, (GATE,), take(FAR_MID, False), 2 + h, min(3 + h, 4))
+            if h == 0:
+                each(1, (GATE,), take(FAR_MID, False), 3, 4)
+            else:
+                each(1, (SIG,), take(FAR_END, False), h - 1, h)
 
     x = feats.at[1]
     for h in every:
@@ -929,12 +990,12 @@
 
     @pl.when(inner)
     def _():
+        each(1, (OUT,), own_in)
         each(1, (GATE,), take(FAR_END), 0, 2)
-        each(1, (OUT,), pass_on)
 
     @pl.when(outer)
     def _():
-        each(1, (SIG,), take(FAR_END, False))
+        each(1, (SIG,), take(FAR_END, False), len(parts) - 1, 4)
 
     for h in every:
         spread_near(x, 1, h)
@@ -950,46 +1011,80 @@
 
     spread_relay(x, 1, 0)
 
+    @pl.when(outer)
+    def _():
+        each(1, (GATE,), take(FAR_END, False), 2, 4)
+
     @pl.when(inner)
     def _():
-        each(1, (OUT,), take(FAR_MID))
-
-    @pl.when(outer)
-    def _():
-        each(1, (GATE,), take(FAR_END, False), 2, 4)
-
-    for k in both_in:
-        ready_all(1, k)
+        for q in range(pieces[OUT]):
+            take(FAR_MID)(1, OUT, q)
+            pass_on(1, OUT, q)
+        each(1, (OUT,), own_other)
+
+    home = lax.div(s, 2) == chip
+    first_near, first_far = jnp.where(home, s, mid2), jnp.where(home, mid2, s)
+    ready_all(1, SIG)
+    ready(1, GATE, FAR_MID)
     for h in every:
         for i, b in enumerate(near_blocks):
-            accumulate(0, 1, b, h, i == 0)
-    spread_relay(x, 1, 1)
-    for h in every:
+            accumulate(0, 1, b, h, i == 0, (SIG,))
+        accumulate(0, 1, first_near, h, True, (GATE,))
+
+    def fold_far(h):
         spread_rest(x, 1, h)
         for b in far_blocks:
             scale(0, 1, x, b, h, False)
-            accumulate(0, 1, b, h, False)
+            accumulate(0, 1, b, h, False, (SIG,))
+        accumulate(0, 1, first_far, h, False, (GATE,))
+
+    fold_far(0)
+    ready(1, GATE, PAIR)
+    ready(1, GATE, FAR_END)
+    spread_relay(x, 1, 1)
+
+    @pl.when(outer)
+    def _():
+        each(1, (OUT,), take(FAR_MID, False), 0, 2)
+
+    for h in every:
+        if h:
+            fold_far(h)
+        for b in (pair, end2):
+            accumulate(0, 1, b, h, False, (GATE,))
         blend(0, h)
         if h == 0:
             send_tail(1)
 
+            @pl.when(outer)
+            def _():
+                each(1, (OUT,), take(FAR_MID, False), 2, 4)
+
             @pl.when(inner)
             def _():
-                each(1, (OUT,), take(FAR_END))
-
-            @pl.when(outer)
-            def _():
-                each(1, (OUT,), take(FAR_MID, False))
+                each(1, (OUT,), take(FAR_END), 0, 2)
+
+            convolve(1, 0, (0,))
         else:
-            convolve(1, h - 1)
+            for late in every[h + 1 : h + 2]:
+                spread_relay(x, 1, late)
+            convolve(1, h - 1, (1,))
             if h + 1 < len(parts):
-                spread_relay(x, 1, h + 1)
+                convolve(1, h, (0,))
+            if h == 1:
+                @pl.when(inner)
+                def _():
+                    each(1, (OUT,), take(FAR_END), 2, 4)
+
+                @pl.when(outer)
+                def _():
+                    each(1, (OUT,), take(FAR_END, False), 0, 2)
     convolve(1, every[-1])
     activate(1, 0)
 
     @pl.when(outer)
     def _():
-        each(1, (OUT,), take(FAR_END, False))
+        each(1, (OUT,), take(FAR_END, False), 2, 4)
 
     for h in every[1:]:
         activate(1, h)
@@ -1078,6 +1173,11 @@
     if folds:
         body = fold_kernel
         scratch = [
+            pltpu.VMEM(norm_gain.shape, BF16),
+            pltpu.VMEM((kernel_taps, layers, local), BF16),
+            pltpu.VMEM(conv_bias.shape, BF16),
+            pltpu.VMEM(ln_gain.shape, BF16),
+            pltpu.VMEM(ln_shift.shape, BF16),
             bank(w_signal), bank(w_gate), bank(w_out),
             pltpu.VMEM((layers, tp, rows, part), BF16),
             pltpu.VMEM((tp, rows, part), BF16),
@@ -1094,7 +1194,7 @@
             pltpu.VMEM((layers, tp, 8, rows), F32),
             pltpu.VMEM((layers, tp, rows, local), BF16),
             pltpu.VMEM((rows, part), BF16),
-            dma(layers, 3), pltpu.SemaphoreType.DMA, pltpu.SemaphoreType.DMA,
+            dma(5), dma(layers, 3), pltpu.SemaphoreType.DMA, pltpu.SemaphoreType.DMA,
             dma(layers, 3, 3), dma(layers, 3, 3), dma(layers, 3, most, 3),
             dma(layers, 3, 3), dma(layers, 3, 3),
             dma(spreads, chips - 1), dma(spreads, count, chips - 1),
@@ -1128,7 +1228,9 @@
             body, (groups, sp, tp, layers, rows, kernel_taps, hp, width, channels)
         ),
         out_shape=jax.ShapeDtypeStruct(stream.shape, BF16),
-        in_specs=[anywhere, inside, anywhere, anywhere, inside, inside, inside, inside, anywhere],
+        in_specs=[anywhere] * 9 if folds else [
+            anywhere, inside, anywhere, anywhere, inside, inside, inside, inside, anywhere,
+        ],
         out_specs=anywhere if folds else inside,
         scratch_shapes=scratch,
         compiler_params=pltpu.CompilerParams(

time: 111 us -> 100 us (0.901); the launches traced: 109 us -> 100 us
  Pallas kernels: 107 us -> 97.9 us
    pallas_call x1, Pallas kernels: 107 us -> 97.9 us  [shards(): pl.pallas_call(functools.partial(body, (groups, sp, tp, layers, rows, ker...]
where the time goes in v3:
time: 100 us
  Pallas kernels  97.9 us (98%)
  local copies, waits for them, and re-layouts  2.06 us (2%)
    pallas_call x1, Pallas kernels, shards(): pl.pallas_call(functools.partial(body, (groups, sp, tp, layers, rows, ker...  97.9 us
    unnamed x1, local copies, waits for them, and re-layouts  2.06 us

profile of v3, /device:TPU:0, one launch (start us, length us, event | category | flops | bytes accessed | tf_op | source)
XLA Modules:
  0.0 100.0 jit_solution(4882089328735177323)
XLA Ops:
  0.0 97.9 %shard_map.91 = bf16[384,1024]{1,0:T(8,128)(2,1)} custom-call(bf16[384,1024]{1,0:T(8,128)(2,1)} %stream.1, bf16[2,4096]{1,0:T(2,128)(2,1)} %gain_in.1, bf16[2,2,4,128,256]{4,3,2,1,0:T(8,128)(2,1)} %bitcast.4, bf16[2,2,4,128,256]{4,3,2,1,0:T(8,128)(2,1)} %bitcast.5, bf16[31,2,256]{2,1,0:T(2,128)(2,1)} %bitcast.7, bf16[2,256]{1,0:T(2,128)(2,1)} %bias_in.1, ...), custom_call_target="tpu_custom_call" | custom-call | tf_op jit(solution)/shard_map/pallas_call | solution.py:1226
  97.9 2.1 %copy.11 = bf16[384,1024]{1,0:T(8,128)(2,1)} copy(bf16[384,1024]{1,0:T(8,128)(2,1)} %shard_map.91) | data formatting | bytes 1572864

commit v4 on v3

--- a/solution.py
+++ b/solution.py
@@ -385,7 +385,7 @@
     result, gain, taps, bias, ln_gain, ln_shift,
     sig_all, gate_all, out_all, feats, far, scaled, squares, acc_sig, acc_gate,
     back, tail, halo, padded, filt, stat_cols, stat_rows, acts,
-    final, small_sem, load_sem, stream_sem, final_sem, z_send, end_send, z_recv, y_send, y_recv,
+    final, small_sem, load_sem, stream_sem, final_sem, z_send, end_send, z_recv, y_send, rest_send, y_recv,
     cross_send, cross_recv, core_send, core_recv,
     far_send, far_recv, back_send, back_recv,
     halo_send, halo_recv, stat_send, stat_recv,
@@ -459,7 +459,7 @@
         ref = banks[k].at[l, where[kind], g, q]
         return pltpu.make_async_remote_copy(
             src_ref=ref, dst_ref=ref,
-            send_sem=sems.at[l, k, spot], recv_sem=z_recv.at[l, k, q, spot],
+            send_sem=sems.at[l, k // OUT], recv_sem=z_recv.at[l, k, q, spot],
             device_id={"sp": to}, device_id_type=MESH,
         )
 
@@ -467,7 +467,7 @@
         ref = banks[k].at[l, where[kind], half, q]
         return pltpu.make_async_remote_copy(
             src_ref=ref, dst_ref=ref,
-            send_sem=sems.at[l, k, spot], recv_sem=y_recv.at[l, k, spot],
+            send_sem=sems.at[l, k // OUT], recv_sem=y_recv.at[l, k, spot],
             device_id=to, device_id_type=MESH,
         )
 
@@ -516,7 +516,7 @@
 
     def share_rest(l, k, q):
         if not direct(l, k, q, pieces[k]):
-            across(l, k, q, PAIR)
+            y_copy(l, k, q, PAIR, g, other_group, rest_send, PAIR).start()
 
     def got(kind):
         return lambda l, k, q: arrived(l, k, q, kind)
@@ -538,9 +538,23 @@
         for kind in (PAIR, FAR_MID, FAR_END):
             ready(l, k, kind)
 
-    def sent(l, k, sems, spot, low=0):
-        ref = banks[k].at[l, s, g, pl.ds(low, pieces[k] - low)]
-        pltpu.make_async_copy(ref, ref, sems.at[l, k, spot]).wait()
+    def sent(sems, pick):
+        for l in range(layers):
+            for kinds in (both_in, (OUT,)):
+                k = kinds[0]
+                count, half = sum(pick(l, k, pieces[k]) for k in kinds), pieces[k]
+                if count == 0:
+                    continue
+                if count % (2 * half) == 0:
+                    ref = banks[k].at[l, pl.ds(0, count // (2 * half))]
+                elif count % half == 0:
+                    ref = banks[k].at[l, pl.ds(0, count // half), 0]
+                else:
+                    ref = banks[k].at[l, 0, 0, pl.ds(0, count)]
+                pltpu.make_async_copy(ref, ref, sems.at[l, k // OUT]).wait()
+
+    def straight(l, k, count):
+        return sum(direct(l, k, q, count) for q in range(count))
 
     def rows_of(h):
         return pl.ds(parts[h][0], parts[h][1])
@@ -952,7 +966,8 @@
 
     @pl.when(inner)
     def _():
-        each(1, (SIG,), take(FAR_END), 0, 3)
+        each(1, (SIG,), take(FAR_END), 0, 1)
+        each(1, (GATE,), pass_on, 0, 1)
 
     @pl.when(outer)
     def _():
@@ -961,10 +976,6 @@
     for h in every:
         spread_relay(acts.at[0], layers, h)
         if h == 0:
-            @pl.when(outer)
-            def _():
-                each(1, (GATE,), take(FAR_MID, False), 2, 3)
-
             ready_all(0, OUT)
         spread_near(acts.at[0], layers, h)
         spread_rest(acts.at[0], layers, h)
@@ -973,14 +984,14 @@
 
         @pl.when(inner)
         def _(h=h):
-            if h == 0:
-                each(1, (SIG,), take(FAR_END), 3, 4)
-            each(1, (GATE,), pass_on, 2 * h, min(2 * h + 2, 4))
+            for q in range(2 * h + 1, min(2 * h + 3, 4)):
+                each(1, (SIG,), take(FAR_END), q, q + 1)
+                each(1, (GATE,), pass_on, q, q + 1)
 
         @pl.when(outer)
         def _(h=h):
             if h == 0:
-                each(1, (GATE,), take(FAR_MID, False), 3, 4)
+                each(1, (GATE,), take(FAR_MID, False), 2, 4)
             else:
                 each(1, (SIG,), take(FAR_END, False), h - 1, h)
 
@@ -1001,35 +1012,8 @@
         spread_near(x, 1, h)
         scale(0, 1, x, mate, h, False)
 
-    @pl.when(inner)
-    def _():
-        each(1, (GATE,), take(FAR_END), 2, 4)
-
-    @pl.when(outer)
-    def _():
-        each(1, (GATE,), take(FAR_END, False), 0, 2)
-
-    spread_relay(x, 1, 0)
-
-    @pl.when(outer)
-    def _():
-        each(1, (GATE,), take(FAR_END, False), 2, 4)
-
-    @pl.when(inner)
-    def _():
-        for q in range(pieces[OUT]):
-            take(FAR_MID)(1, OUT, q)
-            pass_on(1, OUT, q)
-        each(1, (OUT,), own_other)
-
     home = lax.div(s, 2) == chip
     first_near, first_far = jnp.where(home, s, mid2), jnp.where(home, mid2, s)
-    ready_all(1, SIG)
-    ready(1, GATE, FAR_MID)
-    for h in every:
-        for i, b in enumerate(near_blocks):
-            accumulate(0, 1, b, h, i == 0, (SIG,))
-        accumulate(0, 1, first_near, h, True, (GATE,))
 
     def fold_far(h):
         spread_rest(x, 1, h)
@@ -1038,61 +1022,84 @@
             accumulate(0, 1, b, h, False, (SIG,))
         accumulate(0, 1, first_far, h, False, (GATE,))
 
-    fold_far(0)
+    @pl.when(inner)
+    def _():
+        each(1, (GATE,), take(FAR_END), 2, 4)
+
+    for step in range(4):
+        @pl.when(inner)
+        def _(step=step):
+            if step == 0:
+                spread_relay(x, 1, 0)
+            each(1, (OUT,), take(FAR_MID), step, step + 1)
+            each(1, (OUT,), pass_on, step, step + 1)
+            if step == 3:
+                each(1, (OUT,), own_other)
+
+        @pl.when(outer)
+        def _(step=step):
+            each(1, (GATE,), take(FAR_END, False), step, step + 1)
+            if step == 0:
+                spread_relay(x, 1, 0)
+
+        if step == 0:
+            ready(1, GATE, FAR_MID)
+            for h in every:
+                accumulate(0, 1, first_near, h, True, (GATE,))
+        if step == 1:
+            ready_all(1, SIG)
+            for h in every:
+                for i, b in enumerate(near_blocks):
+                    accumulate(0, 1, b, h, i == 0, (SIG,))
+        if step == 2:
+            fold_far(0)
+    def take_out(kind_outer, kind_inner, low, high):
+        @pl.when(outer)
+        def _():
+            each(1, (OUT,), take(kind_outer, False), low, high)
+
+        if kind_inner is not None:
+            @pl.when(inner)
+            def _():
+                each(1, (OUT,), take(kind_inner), low, high)
+
+    spread_relay(x, 1, 1)
+    fold_far(1)
+    take_out(FAR_MID, FAR_END, 0, 1)
     ready(1, GATE, PAIR)
     ready(1, GATE, FAR_END)
-    spread_relay(x, 1, 1)
-
-    @pl.when(outer)
-    def _():
-        each(1, (OUT,), take(FAR_MID, False), 0, 2)
-
+    take_out(FAR_MID, FAR_END, 1, 2)
     for h in every:
-        if h:
+        if h > 1:
+            spread_relay(x, 1, h)
+            convolve(1, h - 1, (0,))
+            take_out(FAR_MID, None, 3, 4)
             fold_far(h)
+            take_out(FAR_END, None, 0, 1)
         for b in (pair, end2):
             accumulate(0, 1, b, h, False, (GATE,))
         blend(0, h)
         if h == 0:
             send_tail(1)
-
-            @pl.when(outer)
-            def _():
-                each(1, (OUT,), take(FAR_MID, False), 2, 4)
-
-            @pl.when(inner)
-            def _():
-                each(1, (OUT,), take(FAR_END), 0, 2)
-
+            take_out(FAR_MID, FAR_END, 2, 3)
             convolve(1, 0, (0,))
         else:
-            for late in every[h + 1 : h + 2]:
-                spread_relay(x, 1, late)
             convolve(1, h - 1, (1,))
-            if h + 1 < len(parts):
-                convolve(1, h, (0,))
             if h == 1:
                 @pl.when(inner)
                 def _():
-                    each(1, (OUT,), take(FAR_END), 2, 4)
-
-                @pl.when(outer)
-                def _():
-                    each(1, (OUT,), take(FAR_END, False), 0, 2)
+                    each(1, (OUT,), take(FAR_END), 3, 4)
+    take_out(FAR_END, None, 1, 2)
     convolve(1, every[-1])
+    take_out(FAR_END, None, 2, 3)
     activate(1, 0)
-
-    @pl.when(outer)
-    def _():
-        each(1, (OUT,), take(FAR_END, False), 2, 4)
-
+    take_out(FAR_END, None, 3, 4)
     for h in every[1:]:
         activate(1, h)
-    spread_relay(acts.at[1], layers + 1, 0)
+    for h in every:
+        spread_relay(acts.at[1], layers + 1, h)
     ready_all(1, OUT)
     for h in every:
-        if h:
-            spread_relay(acts.at[1], layers + 1, h)
         spread_near(acts.at[1], layers + 1, h)
         spread_rest(acts.at[1], layers + 1, h)
         update(1, h)
@@ -1100,32 +1107,19 @@
     @pl.when(outer)
     def _():
         pltpu.make_async_copy(feats.at[0, t], feats.at[0, t], far_send).wait()
-        for l in range(layers):
-            for k in range(3):
-                sent(l, k, z_send, PAIR)
-                count = sum(direct(l, k, q, pieces[k]) for q in range(pieces[k]))
-                sent(l, k, end_send, PAIR, pieces[k] - count)
-                if l or k == OUT:
-                    for kind in (PAIR, FAR_MID, FAR_END):
-                        sent(l, k, y_send, kind)
+        sent(z_send, lambda l, k, n: n)
+        sent(end_send, straight)
+        sent(y_send, lambda l, k, n: 3 * n if l or k == OUT else 0)
 
     @pl.when(inner)
     def _():
         spread_done(feats.at[0], 0)
         spread_done(far, far_n)
         pltpu.make_async_copy(back, back, back_send).wait()
-        for l in range(layers):
-            for k in range(3):
-                sent(l, k, z_send, FAR_MID)
-                sent(l, k, z_send, FAR_END)
-                sent(l, k, y_send, FAR_MID)
-                sent(l, k, y_send, FAR_END)
-                if l or k == OUT:
-                    for spot in (PAIR, FAR_MID, FAR_END):
-                        sent(l, k, end_send, spot)
-                count = sum(direct(l, k, q, pieces[k]) for q in range(pieces[k]))
-                if count < pieces[k]:
-                    sent(l, k, y_send, PAIR, count)
+        sent(z_send, lambda l, k, n: 2 * n)
+        sent(y_send, lambda l, k, n: 2 * n)
+        sent(end_send, lambda l, k, n: 3 * n if l or k == OUT else 0)
+        sent(rest_send, lambda l, k, n: n - straight(l, k, n))
 
     for l in range(layers):
         if l:
@@ -1195,8 +1189,8 @@
             pltpu.VMEM((layers, tp, rows, local), BF16),
             pltpu.VMEM((rows, part), BF16),
             dma(5), dma(layers, 3), pltpu.SemaphoreType.DMA, pltpu.SemaphoreType.DMA,
-            dma(layers, 3, 3), dma(layers, 3, 3), dma(layers, 3, most, 3),
-            dma(layers, 3, 3), dma(layers, 3, 3),
+            dma(layers, 2), dma(layers, 2), dma(layers, 3, most, 3),
+            dma(layers, 2), dma(layers, 2), dma(layers, 3, 3),
             dma(spreads, chips - 1), dma(spreads, count, chips - 1),
             dma(spreads, chips), dma(spreads, count, chips),
             pltpu.SemaphoreType.DMA, dma(count), pltpu.SemaphoreType.DMA, dma(count),

time: 100 us -> 97.2 us (0.972)
  Pallas kernels: 97.9 us -> 95 us
    pallas_call x1, Pallas kernels: 97.9 us -> 95 us  [shards(): pl.pallas_call(functools.partial(body, (groups, sp, tp, layers, rows, ker...]
where the time goes in v4:
time: 97.2 us; the launch traced here: 97 us
  Pallas kernels  95 us (98%)
  local copies, waits for them, and re-layouts  2.06 us (2%)
    pallas_call x1, Pallas kernels, shards(): pl.pallas_call(functools.partial(body, (groups, sp, tp, layers, rows, ker...  95 us
    unnamed x1, local copies, waits for them, and re-layouts  2.06 us

profile of v4, /device:TPU:0, one launch (start us, length us, event | category | flops | bytes accessed | tf_op | source)
XLA Modules:
  0.0 97.0 jit_solution(7559696785143125158)
XLA Ops:
  0.0 95.0 %shard_map.91 = bf16[384,1024]{1,0:T(8,128)(2,1)} custom-call(bf16[384,1024]{1,0:T(8,128)(2,1)} %stream.1, bf16[2,4096]{1,0:T(2,128)(2,1)} %gain_in.1, bf16[2,2,4,128,256]{4,3,2,1,0:T(8,128)(2,1)} %bitcast.4, bf16[2,2,4,128,256]{4,3,2,1,0:T(8,128)(2,1)} %bitcast.5, bf16[31,2,256]{2,1,0:T(2,128)(2,1)} %bitcast.7, bf16[2,256]{1,0:T(2,128)(2,1)} %bias_in.1, ...), custom_call_target="tpu_custom_call" | custom-call | tf_op jit(solution)/shard_map/pallas_call | solution.py:1220
  95.0 2.1 %copy.11 = bf16[384,1024]{1,0:T(8,128)(2,1)} copy(bf16[384,1024]{1,0:T(8,128)(2,1)} %shard_map.91) | data formatting | bytes 1572864

commit v5 on v4

--- a/solution.py
+++ b/solution.py
@@ -385,7 +385,7 @@
     result, gain, taps, bias, ln_gain, ln_shift,
     sig_all, gate_all, out_all, feats, far, scaled, squares, acc_sig, acc_gate,
     back, tail, halo, padded, filt, stat_cols, stat_rows, acts,
-    final, small_sem, load_sem, stream_sem, final_sem, z_send, end_send, z_recv, y_send, rest_send, y_recv,
+    final, partial, small_sem, load_sem, stream_sem, final_sem, z_send, end_send, z_recv, y_send, rest_send, y_recv,
     cross_send, cross_recv, core_send, core_recv,
     far_send, far_recv, back_send, back_recv,
     halo_send, halo_recv, stat_send, stat_recv,
@@ -763,26 +763,22 @@
             final.at[rows_of(h)], result.at[rows_of(h)], final_sem
         )
 
-    def update(l, h):
-        begin, count = parts[h]
+    def update(l, h, blocks, fresh=True, finish=True):
+        at = rows_of(h)
         tile = min(256, part)
-
-        def body(c, carry):
-            at = pl.ds(pl.multiple_of(begin + c * DEEP, DEEP), DEEP)
-            for n in range(part // tile):
-                cut = slice(n * tile, (n + 1) * tile)
-                total = feats[l, t, at, cut].astype(F32)
-                for b in range(tp):
-                    w = out_all[l, b, :, :, :, cut].reshape(local, tile)
-                    total = total + jnp.dot(acts[l, b, at, :], w, preferred_element_type=F32)
-                if l + 1 < layers:
-                    feats[l + 1, t, at, cut] = total.astype(BF16)
-                else:
-                    final[at, cut] = total.astype(BF16)
-            return carry
-
-        lax.fori_loop(0, count // DEEP, body, 0)
-        if l + 1 == layers:
+        for n in range(part // tile):
+            cut = slice(n * tile, (n + 1) * tile)
+            total = feats[l, t, at, cut].astype(F32) if fresh else partial[:, cut]
+            for b in blocks:
+                w = out_all[l, b, :, :, :, cut].reshape(local, tile)
+                total = total + jnp.dot(acts[l, b, at, :], w, preferred_element_type=F32)
+            if not finish:
+                partial[:, cut] = total
+            elif l + 1 < layers:
+                feats[l + 1, t, at, cut] = total.astype(BF16)
+            else:
+                final[at, cut] = total.astype(BF16)
+        if finish and l + 1 == layers:
             write(h).start()
 
     far_n = 2 * layers
@@ -975,11 +971,16 @@
 
     for h in every:
         spread_relay(acts.at[0], layers, h)
-        if h == 0:
-            ready_all(0, OUT)
         spread_near(acts.at[0], layers, h)
         spread_rest(acts.at[0], layers, h)
-        update(0, h)
+        if h == 0:
+            ready(0, OUT, PAIR)
+            ready(0, OUT, FAR_MID)
+            update(0, h, (s, pair, mid2), finish=False)
+            ready(0, OUT, FAR_END)
+            update(0, h, (end2,), fresh=False)
+        else:
+            update(0, h, range(tp))
         spread_start(feats.at[1], 1, h)
 
         @pl.when(inner)
@@ -1016,10 +1017,13 @@
     first_near, first_far = jnp.where(home, s, mid2), jnp.where(home, mid2, s)
 
     def fold_far(h):
-        spread_rest(x, 1, h)
-        for b in far_blocks:
-            scale(0, 1, x, b, h, False)
-            accumulate(0, 1, b, h, False, (SIG,))
+        for c in (core, 1 - core):
+            for i in range(1, chips):
+                b = chip_at(i) + c
+                scale(0, 1, x, b, h, False)
+                accumulate(0, 1, b, h, False, (SIG,))
+            if c is core:
+                spread_rest(x, 1, h)
         accumulate(0, 1, first_far, h, False, (GATE,))
 
     @pl.when(inner)
@@ -1096,13 +1100,22 @@
     take_out(FAR_END, None, 3, 4)
     for h in every[1:]:
         activate(1, h)
-    for h in every:
-        spread_relay(acts.at[1], layers + 1, h)
+    gathered, n = acts.at[1], layers + 1
+    for h in every[:2]:
+        spread_relay(gathered, n, h)
     ready_all(1, OUT)
-    for h in every:
-        spread_near(acts.at[1], layers + 1, h)
-        spread_rest(acts.at[1], layers + 1, h)
-        update(1, h)
+    for h in every[:-1]:
+        spread_near(gathered, n, h)
+        spread_rest(gathered, n, h)
+        update(1, h, range(tp))
+        if h + 2 < len(parts):
+            spread_relay(gathered, n, h + 2)
+    h = every[-1]
+    spread_near(gathered, n, h)
+    early = near_blocks + [chip_at(i) + core for i in range(1, chips)]
+    update(1, h, early, finish=False)
+    spread_rest(gathered, n, h)
+    update(1, h, [chip_at(i) + 1 - core for i in range(1, chips)], fresh=False)
 
     @pl.when(outer)
     def _():
@@ -1188,6 +1201,7 @@
             pltpu.VMEM((layers, tp, 8, rows), F32),
             pltpu.VMEM((layers, tp, rows, local), BF16),
             pltpu.VMEM((rows, part), BF16),
+            pltpu.VMEM((DEEP, part), F32),
             dma(5), dma(layers, 3), pltpu.SemaphoreType.DMA, pltpu.SemaphoreType.DMA,
             dma(layers, 2), dma(layers, 2), dma(layers, 3, most, 3),
             dma(layers, 2), dma(layers, 2), dma(layers, 3, 3),

time: 97.2 us -> 96.6 us (level)
  no operation moved by 1% of the time
where the time goes in v5:
time: 96.6 us; the launch traced here: 96.5 us
  Pallas kernels  94.4 us (98%)
  local copies, waits for them, and re-layouts  2.06 us (2%)
    pallas_call x1, Pallas kernels, shards(): pl.pallas_call(functools.partial(body, (groups, sp, tp, layers, rows, ker...  94.4 us
    unnamed x1, local copies, waits for them, and re-layouts  2.06 us

profile of v5, /device:TPU:0, one launch (start us, length us, event | category | flops | bytes accessed | tf_op | source)
XLA Modules:
  0.0 96.5 jit_solution(10672667114701959156)
XLA Ops:
  0.0 94.4 %shard_map.91 = bf16[384,1024]{1,0:T(8,128)(2,1)} custom-call(bf16[384,1024]{1,0:T(8,128)(2,1)} %stream.1, bf16[2,4096]{1,0:T(2,128)(2,1)} %gain_in.1, bf16[2,2,4,128,256]{4,3,2,1,0:T(8,128)(2,1)} %bitcast.4, bf16[2,2,4,128,256]{4,3,2,1,0:T(8,128)(2,1)} %bitcast.5, bf16[31,2,256]{2,1,0:T(2,128)(2,1)} %bitcast.7, bf16[2,256]{1,0:T(2,128)(2,1)} %bias_in.1, ...), custom_call_target="tpu_custom_call" | custom-call | tf_op jit(solution)/shard_map/pallas_call | solution.py:1234
  94.4 2.1 %copy.11 = bf16[384,1024]{1,0:T(8,128)(2,1)} copy(bf16[384,1024]{1,0:T(8,128)(2,1)} %shard_map.91) | data formatting | bytes 1572864
